TPU v7x, 512 devices: a whole 4x4x16 slice. The times are simulated.
512 devices in a mesh: rep: 2 (over z_hi), fs: 32 (over z_lo, y), tp: 8 (over x, core).
Axes of the slice: x: 4, y: 4, z: 16 (z_hi: 2, z_lo: 8; z = z_hi * 8 + z_lo), core: 2. Of those that a mesh axis runs over, the one named last changes fastest.
Arguments:
- input_activation_entries: bfloat16 [24576, 2048], P(('rep', 'fs')), may hold values from -6 to 6
- premixing_rescale_factor: float32 [2048], replicated, may hold values from 0.1 to 1.9
- probe_weight_table: float32 [2048, 1024], P('fs', 'tp'), may hold values from -0.125 to 0.125
- probe_factor_list: float32 [1024], P('tp'), may hold values from 0.5 to 2
- lookup_weight_table: float32 [2048, 1024], P('fs', 'tp'), may hold values from -0.125 to 0.125
- lookup_factor_list: float32 [1024], P('tp'), may hold values from 0.5 to 2
- forget_weight_table: float32 [2048, 1024], P('fs', 'tp'), may hold values from -0.125 to 0.125
- forget_factor_list: float32 [1024], P('tp'), may hold values from 1 to 8
- forget_shift_term: float32 [1024], P('tp'), may hold values from -3 to 7
- extra_forget_logs: float32 [24576, 8], P(('rep', 'fs'), 'tp'), may hold values from -0.7 to 0
- content_weight_table: float32 [2048, 2048], P('fs', 'tp'), may hold values from -0.125 to 0.125
- content_factor_list: float32 [2048], P('tp'), may hold values from 0.5 to 2
- filter_weight_table: float32 [2048, 2048], P('fs', 'tp'), may hold values from -0.125 to 0.125
- filter_factor_list: float32 [2048], P('tp'), may hold values from 0.5 to 2
- per_group_rescale_factor: float32 [2048], P('tp'), may hold values from 0.1 to 1.9
- emission_weight_table: float32 [2048, 2048], P('tp', 'fs'), may hold values from -0.125 to 0.125
- emission_factor_list: float32 [2048], P('fs'), may hold values from 0.5 to 2
- perceptron_prenorm_factor: float32 [2048], replicated, may hold values from 0.1 to 1.9
- raising_weight_table: float32 [2048, 8192], P('fs', 'tp'), may hold values from -0.125 to 0.125
- raising_factor_list: float32 [8192], P('tp'), may hold values from 0.5 to 2
- lowering_weight_table: float32 [8192, 2048], P('tp', 'fs'), may hold values from -0.0625 to 0.0625
- lowering_factor_list: float32 [2048], P('fs'), may hold values from 0.5 to 2
Outputs:
- layer_out: bfloat16 [24576, 2048], P(('rep', 'fs'))
All inputs are finite; a program needn't handle non-finite values.
Results may differ from a plain program's by a relative error of at most 0.02.
Values may be sent and summed in bfloat16 or wider, within the bound.
No kernel may reach another device: no remote copies, remote signals or barrier semaphores. Data moves between devices by JAX's collectives and lax.ppermute only.
A program may use at most 64 MiB of HBM per device.

v0:
```python
import jax
import jax.numpy as jnp
from jax import lax
from jax.experimental import pallas as pl
from jax.experimental.pallas import tpu as pltpu
from jax.sharding import PartitionSpec as P


EPS = 1e-06
BLOCK = 64
ROWS = 384
D = 2048
BF = jnp.bfloat16
F32 = jnp.float32
HI = lax.Precision.HIGHEST
OFFSETS = (0, -1, 1, -2, 2, -3, 3, 4)
LEVELS = (32, 16, 8, 4, 2, 1)
ZY = ("rep", "fs")
EXTRA = 512
VMEM_LIMIT = 10 * 1024 * 1024


def z_pairs(step):
    return [(z * 4 + y, ((z + step) % 16) * 4 + y) for z in range(16) for y in range(4)]


def y_pairs(mask):
    return [(z * 4 + y, z * 4 + (y ^ mask)) for z in range(16) for y in range(4)]


def z_send(value, step):
    return lax.ppermute(value, ZY, z_pairs(step))


def y_send(value, mask):
    return lax.ppermute(value, ZY, y_pairs(mask))


def x_send(value, mask):
    return lax.ppermute(value, "tp", [(t, t ^ (2 * mask)) for t in range(8)])


def core_swap(value):
    return lax.ppermute(value, "tp", [(t, t ^ 1) for t in range(8)])


def z_gather(own, far_step):
    up, down = own, own
    got = {0: own}
    for k in range(1, 4):
        up = z_send(up, 1)
        down = z_send(down, -1)
        got[-k], got[k] = up, down
    got[4] = z_send(up if far_step > 0 else down, far_step)
    return [got[d] for d in OFFSETS]


def y_gather(own):
    first = y_send(own, 1)
    third = y_send(own, 3)
    cut = own.shape[0] // 2
    return (own, first, y_send(first[:cut], 3), y_send(third[cut:], 1), third)


def y_direct(own):
    far = y_send(own, 2)
    return own, y_send(own, 1), far, y_send(own, 3)


def low_lanes(rows):
    return lax.broadcasted_iota(jnp.int32, (rows, 128), 1) < 64


def turn(tile):
    return pltpu.roll(tile, 64, 1)


def to_a(load, z):
    tiles = []
    for d in OFFSETS:
        base = pl.multiple_of(((z + d) & 7) * 256, 256)
        for t in range(2):
            tiles.append(load(pl.multiple_of(base + 128 * t, 128)))
    return tiles


def b_to_a(tiles, rows):
    low = low_lanes(rows)
    out = []
    for i in range(8):
        j = i // 2
        for t in range(2):
            even, odd = tiles[8 * t + j], tiles[8 * t + 4 + j]
            if i % 2 == 0:
                out.append(jnp.where(low, even, turn(odd)))
            else:
                out.append(jnp.where(low, turn(even), odd))
    return out


def a_to_b(tiles, rows):
    low = low_lanes(rows)
    out = []
    for y in range(4):
        t, h = y >> 1, y & 1
        for j in range(4):
            first, second = tiles[4 * j + t], tiles[4 * j + 2 + t]
            if h == 0:
                out.append(jnp.where(low, first, turn(second)))
            else:
                out.append(jnp.where(low, turn(first), second))
    return out


def cast_kernel(*refs):
    sources, (attention, ffn), held, sems = refs[:10], refs[10:12], refs[12:22], refs[22]
    copies = [pltpu.make_async_copy(s, h, sems.at[n]) for n, (s, h) in enumerate(zip(sources, held))]
    for copy in copies:
        copy.start()
    eye = lax.broadcasted_iota(jnp.int32, (64, 64), 0) == lax.broadcasted_iota(
        jnp.int32, (64, 64), 1
    )

    def column(ref):
        return jnp.sum(jnp.where(eye, ref[...], 0.0), axis=-1, keepdims=True)

    at = 0
    for n in range(5):
        copies[n].wait()
        attention[:, at : at + held[n].shape[1]] = held[n][...].astype(BF)
        at += held[n].shape[1]
    copies[5].wait()
    copies[8].wait()
    attention[:, at:1152] = (held[5][...] * column(held[8])).astype(BF)
    copies[7].wait()
    copies[9].wait()
    low = (held[7][...] * column(held[9])).astype(BF)
    attention[:, 1152:] = low[:, :EXTRA]
    ffn[:, 1024:] = low[:, EXTRA:]
    copies[6].wait()
    ffn[:, :1024] = held[6][...].astype(BF)


def stack_kernel(*refs):
    blocks, (tables_ref, low_ref) = refs[:8], refs[8:]
    for n, ref in enumerate(blocks):
        at = slice(64 * n, 64 * (n + 1))
        tables_ref[at, :] = ref[:, :1152]
        low_ref[at, :] = ref[:, 1152:]


def rows_kernel(where_ref, *refs):
    blocks, out_ref = refs[:4], refs[4]
    for mask, ref in enumerate(blocks):
        out_ref[pl.ds(pl.multiple_of((where_ref[1] ^ mask) * 64, 64), 64), :] = ref[...]


def half_kernel(where_ref, *refs):
    blocks, out_ref = refs[:4], refs[4]
    for mask, ref in enumerate(blocks):
        out_ref[pl.ds(pl.multiple_of((where_ref[3] ^ mask) * 48, 48), 48), :] = ref[...]


def join_kernel(where_ref, keep_ref, got_ref, *outs):
    for mask, ref in enumerate(outs):
        at = pl.ds(pl.multiple_of((where_ref[3] ^ mask) * 48, 48), 48)
        ref[...] = (keep_ref[at, :].astype(F32) + got_ref[at, :].astype(F32)).astype(BF)


def norm_kernel(where_ref, x_ref, gain_ref, out_ref, keep_ref):
    z, y = where_ref[0], where_ref[1]
    gain = gain_ref[...]
    step = 48

    def rows_of(r, carry):
        start = pl.multiple_of(r * step, 16)
        x = x_ref[pl.ds(start, step), :].astype(F32)
        keep_ref[...] = x * lax.rsqrt(jnp.mean(x * x, axis=-1, keepdims=True) + EPS) * gain
        tiles = a_to_b(to_a(lambda s: keep_ref[:, pl.ds(s, 128)], z), step)
        for k, tile in enumerate(tiles):
            place = pl.multiple_of((y ^ (k // 4)) * 512 + 128 * (k % 4), 128)
            out_ref[pl.ds(start, step), pl.ds(place, 128)] = tile.astype(BF)
        return carry

    lax.fori_loop(0, ROWS // step, rows_of, 0)


def spans_and_pairs():
    t = lax.broadcasted_iota(jnp.int32, (BLOCK, BLOCK), 0)
    u = lax.broadcasted_iota(jnp.int32, (BLOCK, BLOCK), 1)
    spans, pairs = [], []
    for h in LEVELS:
        group = (t | (2 * h - 1)) ^ (2 * h - 1)
        edge = group + h
        later = (t & h) != 0
        ahead = (u >= edge) & (u <= t)
        behind = (u > t) & (u < edge)
        spans.append((later & ahead) | (~later & behind))
        pairs.append(later & (u >= group) & (u < edge))
    spans += [u <= t, u > t]
    return jnp.concatenate([jnp.where(m, 1.0, 0.0) for m in spans], axis=0), pairs, u == t


def silu(v):
    return v / (1.0 + jnp.exp(-v))


NT = (((1,), (1,)), ((), ()))
TN = (((0,), (0,)), ((), ()))


def mixing_kernel(
    where_ref,
    x_ref,
    w0_ref,
    w1_ref,
    w2a_ref,
    w2b_ref,
    w3_ref,
    probe_scale,
    lookup_scale,
    forget_scale,
    content_scale,
    gate_scale,
    shift_ref,
    burst_ref,
    gain_ref,
    keep_ref,
    send_ref,
    q_ref,
    k_ref,
    v_ref,
    ld_ref,
    gate_ref,
    att_ref,
    state_ref,
):
    core = where_ref[2]
    parts = (
        (0, 0, 512, w0_ref),
        (1, 0, 512, w1_ref),
        (2, 0, 256, w2a_ref),
        (2, 256, 256, w2b_ref),
        (3, 0, 512, w3_ref),
    )

    def project(lo, hi, scale):
        total = None
        for mask, start, size, ref in parts:
            at = 512 * mask + start
            piece = jnp.dot(
                x_ref[:, at : at + size], ref[:, lo:hi], preferred_element_type=F32
            )
            total = piece if total is None else total + piece
        return total * scale[...]

    q_ref[...] = (silu(project(0, 128, probe_scale)) * 128**-0.5).astype(BF).astype(F32)
    k_ref[...] = silu(project(128, 256, lookup_scale)).astype(BF).astype(F32)
    pre = project(256, 384, forget_scale) + shift_ref[...]
    soft = jnp.minimum(pre, 0.0) - jnp.log1p(jnp.exp(-jnp.abs(pre)))
    eye = lax.broadcasted_iota(jnp.int32, (128, 128), 0) == lax.broadcasted_iota(
        jnp.int32, (128, 128), 1
    )
    for b in range(3):
        at = slice(128 * b, 128 * (b + 1))
        burst = jnp.sum(jnp.where(eye, burst_ref[:, at], 0.0), axis=-1, keepdims=True)
        ld_ref[at, :] = soft[at, :] * (1.0 / 16.0) + burst
    v_ref[...] = silu(project(384, 640, content_scale)).astype(BF)
    gate_ref[...] = silu(project(640, 896, gate_scale))
    spans, pairs, same = spans_and_pairs()
    state_ref[...] = jnp.zeros_like(state_ref)
    for b in range(ROWS // BLOCK):
        at = slice(b * BLOCK, (b + 1) * BLOCK)
        q, k, v = q_ref[at, :], k_ref[at, :], v_ref[at, :]
        reach = jnp.exp(
            jnp.dot(spans, ld_ref[at, :], precision=HI, preferred_element_type=F32)
        )
        scores = jnp.where(same, jnp.sum(q * k, axis=-1, keepdims=True), 0.0)
        for n in range(len(LEVELS)):
            level = reach[n * BLOCK : (n + 1) * BLOCK, :]
            product = lax.dot_general(
                (q * level).astype(BF), (k * level).astype(BF), NT, preferred_element_type=F32
            )
            scores = jnp.where(pairs[n], product, scores)
        n = len(LEVELS)
        into = reach[n * BLOCK : (n + 1) * BLOCK, :]
        rest = reach[(n + 1) * BLOCK : (n + 2) * BLOCK, :]
        state = state_ref[...]
        o = jnp.dot(scores.astype(BF), v, preferred_element_type=F32) + lax.dot_general(
            (q * into).astype(BF), state.astype(BF), NT, preferred_element_type=F32
        )
        state_ref[...] = state * into[BLOCK - 1 :, :] + lax.dot_general(
            v, (k * rest).astype(BF), TN, preferred_element_type=F32
        )
        o = o * lax.rsqrt(jnp.mean(o * o, axis=-1, keepdims=True) + EPS)
        att_ref[at, :] = (o * gain_ref[...] * gate_ref[at, :]).astype(BF)
    half = ROWS // 2
    for ref, which in ((keep_ref, core), (send_ref, 1 - core)):
        rows = att_ref[pl.ds(pl.multiple_of(which * half, half), half), :]
        for mask, start, size, w in parts:
            at = pl.multiple_of((where_ref[1] ^ mask) * 512 + start, 256)
            ref[:, pl.ds(at, size)] = lax.dot_general(
                rows, w[:, 896:1152], NT, preferred_element_type=F32
            ).astype(BF)


def middle_kernel(where_ref, x_ref, gain_ref, *refs):
    parts, (residual_ref, normed_ref) = refs[:4], refs[4:]
    z = where_ref[0]
    rows = 48
    mixed = []
    for k in range(16):
        at = slice(128 * k, 128 * (k + 1))
        total = parts[0][:, at].astype(F32)
        for part in parts[1:]:
            total = total + part[:, at].astype(F32)
        mixed.append(total)
    mixed = b_to_a(mixed, rows)
    own = to_a(lambda s: x_ref[:, pl.ds(s, 128)].astype(F32), z)
    gain = to_a(lambda s: gain_ref[:, pl.ds(s, 128)], z)
    square = jnp.zeros((rows, 1), F32)
    kept = []
    for k in range(16):
        tile = (own[k] + mixed[k]).astype(BF)
        residual_ref[:, 128 * k : 128 * (k + 1)] = tile
        tile = tile.astype(F32)
        kept.append(tile)
        square = square + jnp.sum(tile * tile, axis=-1, keepdims=True)
    factor = lax.rsqrt(square * (1.0 / D) + EPS)
    for k in range(16):
        normed_ref[:, 128 * k : 128 * (k + 1)] = (kept[k] * factor * gain[k]).astype(BF)


def ffn_kernel(where_ref, own_ref, other_ref, scale_ref, *refs):
    lows, refs = refs[:4], refs[4:]
    pieces, (keep_ref, send_ref, hidden_ref, part_ref) = refs[:8], refs[8:]
    for half, ref in ((0, own_ref), (1, other_ref)):
        for lo in range(0, 1024, 256):
            total = None
            for i, piece in enumerate(pieces):
                part = jnp.dot(
                    ref[:, 256 * i : 256 * (i + 1)],
                    piece[:, lo : lo + 256],
                    preferred_element_type=F32,
                )
                total = part if total is None else total + part
            value = jnp.maximum(total * scale_ref[:, lo : lo + 256], 0.0)
            hidden_ref[half, :, lo : lo + 256] = (value * value).astype(BF)
    rows = ROWS // 2
    low = low_lanes(rows)
    for half, ref in ((1, send_ref), (0, keep_ref)):
        for y in range(4):
            part_ref[where_ref[1] ^ y] = lax.dot_general(
                hidden_ref[half, :, :EXTRA], lows[y][...], NT, preferred_element_type=F32
            )
        for i, piece in enumerate(pieces):
            total = lax.dot_general(
                hidden_ref[half, :, EXTRA:], piece[:, 1024:], NT, preferred_element_type=F32
            )
            at = slice(128 * (i // 2), 128 * (i // 2 + 1))
            for t in range(2):
                even, odd = part_ref[2 * t, :, at], part_ref[2 * t + 1, :, at]
                if i % 2 == 0:
                    extra = jnp.where(low, even, turn(odd))
                else:
                    extra = jnp.where(low, turn(even), odd)
                ref[:, 256 * i + 128 * t : 256 * i + 128 * (t + 1)] = (
                    total[:, 128 * t : 128 * (t + 1)] + extra
                ).astype(BF)


def last_kernel(where_ref, residual_ref, *refs):
    parts, out_ref = refs[:4], refs[4]
    for i, d in enumerate(OFFSETS):
        base = pl.multiple_of(((where_ref[0] + d) & 7) * 256, 256)
        at = slice(256 * i, 256 * (i + 1))
        total = parts[0][:, at].astype(F32)
        for part in parts[1:]:
            total = total + part[:, at].astype(F32)
        out_ref[:, pl.ds(base, 256)] = (residual_ref[:, at].astype(F32) + total).astype(BF)


def place_own_kernel(where_ref, own_ref, out_ref, sem):
    half = ROWS // 2
    start = pl.multiple_of(where_ref[2] * half, half)
    copy = pltpu.make_async_copy(own_ref, out_ref.at[pl.ds(start, half), :], sem)
    copy.start()
    copy.wait()


def place_other_kernel(where_ref, other_ref, held_ref, out_ref, sem):
    half = ROWS // 2
    start = pl.multiple_of((1 - where_ref[2]) * half, half)
    copy = pltpu.make_async_copy(other_ref, out_ref.at[pl.ds(start, half), :], sem)
    copy.start()
    copy.wait()


def near(value):
    return pltpu.with_memory_space_constraint(value, pltpu.VMEM)


def call(kernel, outs, scratch, *args):
    vmem = pl.BlockSpec(memory_space=pltpu.VMEM)
    smem = pl.BlockSpec(memory_space=pltpu.SMEM)
    return pl.pallas_call(
        kernel,
        out_shape=[pltpu.VMEM(s, t) for s, t in outs],
        in_specs=[smem if a.dtype == jnp.int32 else vmem for a in args],
        out_specs=[vmem] * len(outs),
        scratch_shapes=[pltpu.VMEM(s, t) for s, t in scratch],
        compiler_params=pltpu.CompilerParams(vmem_limit_bytes=VMEM_LIMIT),
    )(*args)


def place(where, own, other):
    vmem = pl.BlockSpec(memory_space=pltpu.VMEM)
    smem = pl.BlockSpec(memory_space=pltpu.SMEM)
    far = pl.BlockSpec(memory_space=pl.ANY)
    shape = jax.ShapeDtypeStruct((ROWS, D), BF)
    held = pl.pallas_call(
        place_own_kernel,
        out_shape=shape,
        in_specs=[smem, vmem],
        out_specs=far,
        scratch_shapes=[pltpu.SemaphoreType.DMA],
        compiler_params=pltpu.CompilerParams(vmem_limit_bytes=VMEM_LIMIT),
        name="place_own",
    )(where, near(own))
    return pl.pallas_call(
        place_other_kernel,
        out_shape=shape,
        in_specs=[smem, vmem, far],
        out_specs=far,
        scratch_shapes=[pltpu.SemaphoreType.DMA],
        input_output_aliases={2: 0},
        compiler_params=pltpu.CompilerParams(vmem_limit_bytes=VMEM_LIMIT),
        name="place_other",
    )(where, near(other), held)


def body(
    x,
    pre_gain,
    w_probe,
    s_probe,
    w_lookup,
    s_lookup,
    w_forget,
    s_forget,
    shift,
    burst,
    w_content,
    s_content,
    w_filter,
    s_filter,
    head_gain,
    w_emission,
    s_emission,
    mlp_gain,
    w_raising,
    s_raising,
    w_lowering,
    s_lowering,
):
    fs = lax.axis_index("fs")
    tp = lax.axis_index("tp")
    where = jnp.stack([fs >> 2, fs & 3, tp & 1, tp >> 1]).astype(jnp.int32)
    tables = (
        w_probe,
        w_lookup,
        w_forget,
        w_content,
        w_filter,
        w_emission.T,
        w_raising,
        w_lowering.T,
        s_emission[None, :],
        s_lowering[None, :],
    )
    vmem = pl.BlockSpec(memory_space=pltpu.VMEM)
    far = pl.BlockSpec(memory_space=pl.ANY)
    attention, ffn = pl.pallas_call(
        cast_kernel,
        out_shape=[pltpu.VMEM((64, 1152 + EXTRA), BF), pltpu.VMEM((64, 2048 - EXTRA), BF)],
        in_specs=[far] * 10,
        out_specs=[vmem] * 2,
        scratch_shapes=[pltpu.VMEM(w.shape, F32) for w in tables]
        + [pltpu.SemaphoreType.DMA((10,))],
        compiler_params=pltpu.CompilerParams(vmem_limit_bytes=VMEM_LIMIT),
        name="cast",
    )(
        *(pltpu.with_memory_space_constraint(w, pltpu.HBM) for w in tables)
    )
    along_z, low_z = call(
        stack_kernel,
        [((512, 1152), BF), ((512, EXTRA), BF)],
        [],
        *(near(b) for b in z_gather(attention, 1)),
    )
    tables = y_gather(along_z)
    extra = y_direct(low_z)
    (along_y,) = call(
        rows_kernel, [((256, 2048 - EXTRA), BF)], [], where, *(near(b) for b in y_direct(ffn))
    )
    pieces = z_gather(along_y, 1)

    (normed,) = call(norm_kernel, [((ROWS, D), BF)], [((48, D), F32)], where, x, pre_gain[None, :])
    keep, send = call(
        mixing_kernel,
        [((ROWS // 2, D), BF)] * 2,
        [
            ((ROWS, 128), F32),
            ((ROWS, 128), F32),
            ((ROWS, 256), BF),
            ((ROWS, 128), F32),
            ((ROWS, 256), F32),
            ((ROWS, 256), BF),
            ((256, 128), F32),
        ],
        where,
        near(normed),
        *(near(t) for t in tables),
        s_probe[None, :],
        s_lookup[None, :],
        s_forget[None, :],
        s_content[None, :],
        s_filter[None, :],
        shift[None, :],
        burst.T,
        head_gain[None, :],
    )

    piece = ((48, D), BF)

    def reduce_rows(keep, send):
        own, *others = call(join_kernel, [piece] * 4, [], where, near(keep), near(core_swap(send)))
        got = {m: x_send(others[m - 1], m) for m in (2, 1, 3)}
        return near(own), near(got[1]), near(got[2]), near(got[3])

    def spread_rows(own):
        got = {m: x_send(own, m) for m in (2, 1, 3)}
        (half,) = call(
            half_kernel,
            [((ROWS // 2, D), BF)],
            [],
            where,
            near(own),
            near(got[1]),
            near(got[2]),
            near(got[3]),
        )
        return half, core_swap(half)

    own_rows = lax.dynamic_slice_in_dim(x, where[2] * 192 + where[3] * 48, 48, 0)
    residual, normed_share = call(
        middle_kernel, [piece] * 2, [], where, own_rows, mlp_gain[None, :], *reduce_rows(keep, send)
    )
    own, other = spread_rows(normed_share)
    keep, send = call(
        ffn_kernel,
        [((ROWS // 2, D), BF)] * 2,
        [((2, ROWS // 2, 1024), BF), ((4, ROWS // 2, 512), F32)],
        where,
        near(own),
        near(other),
        s_raising[None, :],
        *(near(e) for e in extra),
        *(near(p) for p in pieces),
    )
    (share,) = call(last_kernel, [piece], [], where, near(residual), *reduce_rows(keep, send))
    return place(where, *spread_rows(share))


def solution(mesh):
    return jax.shard_map(
        body,
        mesh=mesh,
        in_specs=(
            P(("rep", "fs"), None),
            P(),
            P("fs", "tp"),
            P("tp"),
            P("fs", "tp"),
            P("tp"),
            P("fs", "tp"),
            P("tp"),
            P("tp"),
            P(("rep", "fs"), "tp"),
            P("fs", "tp"),
            P("tp"),
            P("fs", "tp"),
            P("tp"),
            P("tp"),
            P("tp", "fs"),
            P("fs"),
            P(),
            P("fs", "tp"),
            P("tp"),
            P("tp", "fs"),
            P("fs"),
        ),
        out_specs=P(("rep", "fs"), None),
        check_vma=False,
    )
```

profile of v0, /device:TPU:1, one launch (start us, length us, event | category | flops | bytes accessed | tf_op | source)
XLA Modules:
  0.0 259.3 jit_solution(13490805253267195366)
XLA Ops:
  0.0 1.4 cast.1
  1.4 4.4 %collective-permute-start = (bf16[64,1664]{1,0:T(8,128)(2,1)S(1)}, bf16[64,1664]{1,0:T(8,128)(2,1)S(1)}, u32[]{:S(2)}, u32[]{:S(2)}) collective-permute-start(bf16[64,1664]{1,0:T(8,128)(2,1)S(1)} %get-tuple-element.23.refs_0_), channel_id=1, source_target_pairs={{0,32},{8,40},{16,48},{24,56},{32,64},{40,72},{48,80},{56,88},{64,... | collective-permute-start | bytes 638984 | tf_op jit(solution)/shard_map/ppermute | solution.py:32
  5.8 9.5 %collective-permute-start.1 = (bf16[64,1664]{1,0:T(8,128)(2,1)S(1)}, bf16[64,1664]{1,0:T(8,128)(2,1)S(1)}, u32[]{:S(2)}, u32[]{:S(2)}) collective-permute-start(bf16[64,1664]{1,0:T(8,128)(2,1)S(1)} %get-tuple-element.23.refs_0_), channel_id=1, source_target_pairs={{0,480},{8,488},{16,496},{24,504},{32,0},{40,8},{48,16},{56,24},{6... | collective-permute-start | bytes 638984 | tf_op jit(solution)/shard_map/ppermute | solution.py:32
  15.3 3.0 %collective-permute-done.refs_1_ = bf16[64,1664]{1,0:T(8,128)(2,1)S(1)} collective-permute-done((bf16[64,1664]{1,0:T(8,128)(2,1)S(1)}, bf16[64,1664]{1,0:T(8,128)(2,1)S(1)}, u32[]{:S(2)}, u32[]{:S(2)}) %collective-permute-start) | collective-permute-done | bytes 213024 | tf_op jit(solution)/shard_map/ppermute | solution.py:32
  18.3 1.9 collective-permute-start.2
  20.2 4.6 %collective-permute-start.3 = (bf16[64,1664]{1,0:T(8,128)(2,1)S(1)}, bf16[64,1664]{1,0:T(8,128)(2,1)S(1)}, u32[]{:S(2)}, u32[]{:S(2)}) collective-permute-start(bf16[64,1664]{1,0:T(8,128)(2,1)S(1)} %collective-permute-done.1.refs_2_), channel_id=1, source_target_pairs={{0,480},{8,488},{16,496},{24,504},{32,0},{40,8},{48,16},{56,24},{6... | collective-permute-start | bytes 638984 | tf_op jit(solution)/shard_map/ppermute | solution.py:32
  24.8 2.1 collective-permute-done.2.refs_3_
  26.9 1.9 collective-permute-start.4
  28.9 4.6 %collective-permute-start.5 = (bf16[64,1664]{1,0:T(8,128)(2,1)S(1)}, bf16[64,1664]{1,0:T(8,128)(2,1)S(1)}, u32[]{:S(2)}, u32[]{:S(2)}) collective-permute-start(bf16[64,1664]{1,0:T(8,128)(2,1)S(1)} %collective-permute-done.3.refs_4_), channel_id=1, source_target_pairs={{0,480},{8,488},{16,496},{24,504},{32,0},{40,8},{48,16},{56,24},{6... | collective-permute-start | bytes 638984 | tf_op jit(solution)/shard_map/ppermute | solution.py:32
  33.4 1.3 collective-permute-done.4.refs_5_
  34.7 1.9 collective-permute-start.6
  36.6 5.9 %collective-permute-done.6.refs_7_ = bf16[64,1664]{1,0:T(8,128)(2,1)S(1)} collective-permute-done((bf16[64,1664]{1,0:T(8,128)(2,1)S(1)}, bf16[64,1664]{1,0:T(8,128)(2,1)S(1)}, u32[]{:S(2)}, u32[]{:S(2)}) %collective-permute-start.6) | collective-permute-done | bytes 213024 | tf_op jit(solution)/shard_map/ppermute | solution.py:32
  42.5 1.1 shard_map.209
  44.4 3.2 %collective-permute-start.7 = (bf16[512,1152]{1,0:T(8,128)(2,1)}, bf16[512,1152]{1,0:T(8,128)(2,1)S(1)}, u32[]{:S(2)}, u32[]{:S(2)}) collective-permute-start(bf16[512,1152]{1,0:T(8,128)(2,1)} %get-tuple-element.24.w0_ref), channel_id=1, source_target_pairs={{0,8},{8,0},{16,24},{24,16},{32,40},{40,32},{48,56},{56,48},{64,72... | collective-permute-start | bytes 3538952 | tf_op jit(solution)/shard_map/ppermute | solution.py:36
  47.6 3.8 %collective-permute-start.9 = (bf16[512,1152]{1,0:T(8,128)(2,1)}, bf16[512,1152]{1,0:T(8,128)(2,1)S(1)}, u32[]{:S(2)}, u32[]{:S(2)}) collective-permute-start(bf16[512,1152]{1,0:T(8,128)(2,1)} %get-tuple-element.24.w0_ref), channel_id=1, source_target_pairs={{0,24},{8,16},{16,8},{24,0},{32,56},{40,48},{48,40},{56,32},{64,88... | collective-permute-start | bytes 3538952 | tf_op jit(solution)/shard_map/ppermute | solution.py:36
  51.5 2.3 collective-permute-start.22
  53.8 3.5 %collective-permute-start.23 = (bf16[64,1536]{1,0:T(8,128)(2,1)S(1)}, bf16[64,1536]{1,0:T(8,128)(2,1)S(1)}, u32[]{:S(2)}, u32[]{:S(2)}) collective-permute-start(bf16[64,1536]{1,0:T(8,128)(2,1)S(1)} %get-tuple-element.34.refs_0_), channel_id=1, source_target_pairs={{0,16},{8,24},{16,0},{24,8},{32,48},{40,56},{48,32},{56,40},{64,80... | collective-permute-start | bytes 589832 | tf_op jit(solution)/shard_map/ppermute | solution.py:36
  57.2 3.8 %collective-permute-start.24 = (bf16[64,1536]{1,0:T(8,128)(2,1)S(1)}, bf16[64,1536]{1,0:T(8,128)(2,1)S(1)}, u32[]{:S(2)}, u32[]{:S(2)}) collective-permute-start(bf16[64,1536]{1,0:T(8,128)(2,1)S(1)} %get-tuple-element.34.refs_0_), channel_id=1, source_target_pairs={{0,24},{8,16},{16,8},{24,0},{32,56},{40,48},{48,40},{56,32},{64,88... | collective-permute-start | bytes 589832 | tf_op jit(solution)/shard_map/ppermute | solution.py:36
  61.1 12.7 %collective-permute-done.22.refs_1_ = bf16[64,1536]{1,0:T(8,128)(2,1)S(1)} collective-permute-done((bf16[64,1536]{1,0:T(8,128)(2,1)S(1)}, bf16[64,1536]{1,0:T(8,128)(2,1)S(1)}, u32[]{:S(2)}, u32[]{:S(2)}) %collective-permute-start.22) | collective-permute-done | bytes 196640 | tf_op jit(solution)/shard_map/ppermute | solution.py:36
  73.9 6.4 %collective-permute-done.23.refs_2_ = bf16[64,1536]{1,0:T(8,128)(2,1)S(1)} collective-permute-done((bf16[64,1536]{1,0:T(8,128)(2,1)S(1)}, bf16[64,1536]{1,0:T(8,128)(2,1)S(1)}, u32[]{:S(2)}, u32[]{:S(2)}) %collective-permute-start.23) | collective-permute-done | bytes 196640 | tf_op jit(solution)/shard_map/ppermute | solution.py:36
  84.1 2.1 collective-permute-start.25
  86.2 3.0 %collective-permute-start.8 = (bf16[256,1152]{1,0:T(8,128)(2,1)S(1)}, bf16[256,1152]{1,0:T(8,128)(2,1)S(1)}, u32[]{:S(2)}, u32[]{:S(2)}) collective-permute-start(bf16[256,1152]{1,0:T(8,128)(2,1)S(1)} %slice.8), channel_id=1, source_target_pairs={{0,24},{8,16},{16,8},{24,0},{32,56},{40,48},{48,40},{56,32},{64,88... | collective-permute-start | bytes 1769480 | tf_op jit(solution)/shard_map/ppermute | solution.py:36
  89.3 1.9 collective-permute-start.10
  91.2 4.6 %collective-permute-start.26 = (bf16[256,1536]{1,0:T(8,128)(2,1)S(1)}, bf16[256,1536]{1,0:T(8,128)(2,1)}, u32[]{:S(2)}, u32[]{:S(2)}) collective-permute-start(bf16[256,1536]{1,0:T(8,128)(2,1)S(1)} %shard_map.214.refs_4_), channel_id=1, source_target_pairs={{0,480},{8,488},{16,496},{24,504},{32,0},{40,8},{48,16},{56,24},{6... | collective-permute-start | bytes 2359304 | tf_op jit(solution)/shard_map/ppermute | solution.py:32
  95.8 3.8 %collective-permute-done.25.refs_5_ = bf16[256,1536]{1,0:T(8,128)(2,1)S(1)} collective-permute-done((bf16[256,1536]{1,0:T(8,128)(2,1)S(1)}, bf16[256,1536]{1,0:T(8,128)(2,1)S(1)}, u32[]{:S(2)}, u32[]{:S(2)}) %collective-permute-start.25) | collective-permute-done | bytes 786464 | tf_op jit(solution)/shard_map/ppermute | solution.py:32
  99.6 1.9 collective-permute-start.27
  101.6 2.7 %shard_map.208.x_ref = bf16[384,2048]{1,0:T(8,128)(2,1)S(1)} custom-call(s32[4]{0:T(128)S(1)} %pad_add_fusion.where_ref, bf16[384,2048]{1,0:T(8,128)(2,1)S(1)} %copy-done, f32[1,2048]{1,0:T(1,128)S(1)} %bitcast.19), custom_call_target="tpu_custom_call" | custom-call | tf_op jit(solution)/shard_map/pallas_call | solution.py:406
  104.5 8.2 %shard_map.210 = (bf16[192,2048]{1,0:T(8,128)(2,1)S(1)}, bf16[192,2048]{1,0:T(8,128)(2,1)S(1)}) custom-call(s32[4]{0:T(128)S(1)} %pad_add_fusion.where_ref, bf16[384,2048]{1,0:T(8,128)(2,1)S(1)} %shard_map.208.x_ref, bf16[512,1152]{1,0:T(8,128)(2,1)} %get-tuple-element.24.w0_ref, bf16[512,1152]{1,0:T(8,128)(2,1)S(1)} %collective-permute-done.7.w1_ref, ...), custom_call_target="tpu_custom_call" | custom-call | tf_op jit(solution)/shard_map/pallas_call | solution.py:406
  112.7 11.1 %collective-permute-start.11 = (bf16[192,2048]{1,0:T(8,128)(2,1)S(1)}, bf16[192,2048]{1,0:T(8,128)(2,1)S(1)}, u32[]{:S(2)}, u32[]{:S(2)}) collective-permute-start(bf16[192,2048]{1,0:T(8,128)(2,1)S(1)} %get-tuple-element.26), channel_id=1, source_target_pairs={{0,1},{1,0},{2,3},{3,2},{4,5},{5,4},{6,7},{7,6},{8,9},{9,8},{10,11... | collective-permute-start | bytes 2359304 | tf_op jit(solution)/shard_map/ppermute | solution.py:44
  123.8 4.9 %collective-permute-start.28 = (bf16[256,1536]{1,0:T(8,128)(2,1)}, bf16[256,1536]{1,0:T(8,128)(2,1)S(1)}, u32[]{:S(2)}, u32[]{:S(2)}) collective-permute-start(bf16[256,1536]{1,0:T(8,128)(2,1)} %collective-permute-done.26.refs_6_), channel_id=1, source_target_pairs={{0,480},{8,488},{16,496},{24,504},{32,0},{40,8},{48,16},{56,24},{6... | collective-permute-start | bytes 2359304 | tf_op jit(solution)/shard_map/ppermute | solution.py:32
  128.7 1.9 collective-permute-start.29
  130.6 1.3 shard_map.211
  133.3 3.2 %collective-permute-start.12 = (bf16[48,2048]{1,0:T(8,128)(2,1)}, bf16[48,2048]{1,0:T(8,128)(2,1)S(1)}, u32[]{:S(2)}, u32[]{:S(2)}) collective-permute-start(bf16[48,2048]{1,0:T(8,128)(2,1)} %get-tuple-element.28), channel_id=1, source_target_pairs={{0,2},{1,3},{2,0},{3,1},{4,6},{5,7},{6,4},{7,5},{8,10},{9,11},{10,... | collective-permute-start | bytes 589832 | tf_op jit(solution)/shard_map/ppermute | solution.py:40
  136.6 2.1 collective-permute-start.19
  138.7 4.4 %collective-permute-start.13 = (bf16[48,2048]{1,0:T(8,128)(2,1)}, bf16[48,2048]{1,0:T(8,128)(2,1)S(1)}, u32[]{:S(2)}, u32[]{:S(2)}) collective-permute-start(bf16[48,2048]{1,0:T(8,128)(2,1)} %copy-done.21), channel_id=1, source_target_pairs={{0,4},{1,5},{2,6},{3,7},{4,0},{5,1},{6,2},{7,3},{8,12},{9,13},{10,... | collective-permute-start | bytes 589832 | tf_op jit(solution)/shard_map/ppermute | solution.py:40
  143.0 3.1 %collective-permute-start.14 = (bf16[48,2048]{1,0:T(8,128)(2,1)}, bf16[48,2048]{1,0:T(8,128)(2,1)S(1)}, u32[]{:S(2)}, u32[]{:S(2)}) collective-permute-start(bf16[48,2048]{1,0:T(8,128)(2,1)} %copy-done.20), channel_id=1, source_target_pairs={{0,6},{1,7},{2,4},{3,5},{4,2},{5,3},{6,0},{7,1},{8,14},{9,15},{10,... | collective-permute-start | bytes 589832 | tf_op jit(solution)/shard_map/ppermute | solution.py:40
  148.2 4.1 %collective-permute-done.14.refs_3_ = bf16[48,2048]{1,0:T(8,128)(2,1)S(1)} collective-permute-done((bf16[48,2048]{1,0:T(8,128)(2,1)}, bf16[48,2048]{1,0:T(8,128)(2,1)S(1)}, u32[]{:S(2)}, u32[]{:S(2)}) %collective-permute-start.14) | collective-permute-done | bytes 196640 | tf_op jit(solution)/shard_map/ppermute | solution.py:40
  153.1 3.3 %collective-permute-start.15 = (bf16[48,2048]{1,0:T(8,128)(2,1)S(1)}, bf16[48,2048]{1,0:T(8,128)(2,1)S(1)}, u32[]{:S(2)}, u32[]{:S(2)}) collective-permute-start(bf16[48,2048]{1,0:T(8,128)(2,1)S(1)} %get-tuple-element.32.refs_0_), channel_id=1, source_target_pairs={{0,2},{1,3},{2,0},{3,1},{4,6},{5,7},{6,4},{7,5},{8,10},{9,11},{10,... | collective-permute-start | bytes 589832 | tf_op jit(solution)/shard_map/ppermute | solution.py:40
  156.4 4.1 %collective-permute-start.16 = (bf16[48,2048]{1,0:T(8,128)(2,1)S(1)}, bf16[48,2048]{1,0:T(8,128)(2,1)S(1)}, u32[]{:S(2)}, u32[]{:S(2)}) collective-permute-start(bf16[48,2048]{1,0:T(8,128)(2,1)S(1)} %get-tuple-element.32.refs_0_), channel_id=1, source_target_pairs={{0,4},{1,5},{2,6},{3,7},{4,0},{5,1},{6,2},{7,3},{8,12},{9,13},{10,... | collective-permute-start | bytes 589832 | tf_op jit(solution)/shard_map/ppermute | solution.py:40
  160.5 2.2 collective-permute-start.17
  162.8 4.5 %collective-permute-start.30 = (bf16[256,1536]{1,0:T(8,128)(2,1)S(1)}, bf16[256,1536]{1,0:T(8,128)(2,1)S(1)}, u32[]{:S(2)}, u32[]{:S(2)}) collective-permute-start(bf16[256,1536]{1,0:T(8,128)(2,1)S(1)} %collective-permute-done.28.refs_8_), channel_id=1, source_target_pairs={{0,480},{8,488},{16,496},{24,504},{32,0},{40,8},{48,16},{56,24},{6... | collective-permute-start | bytes 2359304 | tf_op jit(solution)/shard_map/ppermute | solution.py:32
  167.3 1.9 collective-permute-start.31
  169.3 3.1 %collective-permute-done.17.refs_3_ = bf16[48,2048]{1,0:T(8,128)(2,1)S(1)} collective-permute-done((bf16[48,2048]{1,0:T(8,128)(2,1)S(1)}, bf16[48,2048]{1,0:T(8,128)(2,1)S(1)}, u32[]{:S(2)}, u32[]{:S(2)}) %collective-permute-start.17) | collective-permute-done | bytes 196640 | tf_op jit(solution)/shard_map/ppermute | solution.py:40
  172.9 2.4 collective-permute-start.18
  175.4 5.5 %collective-permute-start.20 = (bf16[512,512]{1,0:T(8,128)(2,1)S(1)}, bf16[512,512]{1,0:T(8,128)(2,1)S(1)}, u32[]{:S(2)}, u32[]{:S(2)}) collective-permute-start(bf16[512,512]{1,0:T(8,128)(2,1)S(1)} %copy-done.4), channel_id=1, source_target_pairs={{0,16},{8,24},{16,0},{24,8},{32,48},{40,56},{48,32},{56,40},{64,80... | collective-permute-start | bytes 1572872 | tf_op jit(solution)/shard_map/ppermute | solution.py:36
  180.9 2.8 %collective-permute-start.21 = (bf16[512,512]{1,0:T(8,128)(2,1)S(1)}, bf16[512,512]{1,0:T(8,128)(2,1)S(1)}, u32[]{:S(2)}, u32[]{:S(2)}) collective-permute-start(bf16[512,512]{1,0:T(8,128)(2,1)S(1)} %copy-done.4), channel_id=1, source_target_pairs={{0,24},{8,16},{16,8},{24,0},{32,56},{40,48},{48,40},{56,32},{64,88... | collective-permute-start | bytes 1572872 | tf_op jit(solution)/shard_map/ppermute | solution.py:36
  183.8 9.4 %collective-permute-done.20.refs_2_ = bf16[512,512]{1,0:T(8,128)(2,1)S(1)} collective-permute-done((bf16[512,512]{1,0:T(8,128)(2,1)S(1)}, bf16[512,512]{1,0:T(8,128)(2,1)S(1)}, u32[]{:S(2)}, u32[]{:S(2)}) %collective-permute-start.20) | collective-permute-done | bytes 524320 | tf_op jit(solution)/shard_map/ppermute | solution.py:36
  193.2 11.3 %collective-permute-done.21.refs_3_ = bf16[512,512]{1,0:T(8,128)(2,1)S(1)} collective-permute-done((bf16[512,512]{1,0:T(8,128)(2,1)S(1)}, bf16[512,512]{1,0:T(8,128)(2,1)S(1)}, u32[]{:S(2)}, u32[]{:S(2)}) %collective-permute-start.21) | collective-permute-done | bytes 524320 | tf_op jit(solution)/shard_map/ppermute | solution.py:36
  204.6 6.1 %shard_map.215 = (bf16[192,2048]{1,0:T(8,128)(2,1)S(1)}, bf16[192,2048]{1,0:T(8,128)(2,1)S(1)}) custom-call(s32[4]{0:T(128)S(1)} %pad_add_fusion.where_ref, bf16[192,2048]{1,0:T(8,128)(2,1)S(1)} %shard_map.213.own_ref, bf16[192,2048]{1,0:T(8,128)(2,1)S(1)} %collective-permute-done.18.other_ref, f32[1,1024]{1,0:T(1,128)S(1)} %bitcast.21, ...), custom_call_target="tpu_custom_call" | custom-call | tf_op jit(solution)/shard_map/pallas_call | solution.py:406
  210.7 2.4 collective-permute-start.32
  213.1 1.9 collective-permute-done.32.got_ref
  215.7 2.2 collective-permute-start.33
  217.9 3.2 %collective-permute-start.34 = (bf16[48,2048]{1,0:T(8,128)(2,1)S(1)}, bf16[48,2048]{1,0:T(8,128)(2,1)S(1)}, u32[]{:S(2)}, u32[]{:S(2)}) collective-permute-start(bf16[48,2048]{1,0:T(8,128)(2,1)S(1)} %get-tuple-element.39), channel_id=1, source_target_pairs={{0,4},{1,5},{2,6},{3,7},{4,0},{5,1},{6,2},{7,3},{8,12},{9,13},{10,... | collective-permute-start | bytes 589832 | tf_op jit(solution)/shard_map/ppermute | solution.py:40
  221.1 4.2 %collective-permute-start.35 = (bf16[48,2048]{1,0:T(8,128)(2,1)S(1)}, bf16[48,2048]{1,0:T(8,128)(2,1)S(1)}, u32[]{:S(2)}, u32[]{:S(2)}) collective-permute-start(bf16[48,2048]{1,0:T(8,128)(2,1)S(1)} %get-tuple-element.40), channel_id=1, source_target_pairs={{0,6},{1,7},{2,4},{3,5},{4,2},{5,3},{6,0},{7,1},{8,14},{9,15},{10,... | collective-permute-start | bytes 589832 | tf_op jit(solution)/shard_map/ppermute | solution.py:40
  225.3 2.9 %collective-permute-done.34.refs_2_ = bf16[48,2048]{1,0:T(8,128)(2,1)S(1)} collective-permute-done((bf16[48,2048]{1,0:T(8,128)(2,1)S(1)}, bf16[48,2048]{1,0:T(8,128)(2,1)S(1)}, u32[]{:S(2)}, u32[]{:S(2)}) %collective-permute-start.34) | collective-permute-done | bytes 196640 | tf_op jit(solution)/shard_map/ppermute | solution.py:40
  228.2 4.8 %collective-permute-done.35.refs_3_ = bf16[48,2048]{1,0:T(8,128)(2,1)S(1)} collective-permute-done((bf16[48,2048]{1,0:T(8,128)(2,1)S(1)}, bf16[48,2048]{1,0:T(8,128)(2,1)S(1)}, u32[]{:S(2)}, u32[]{:S(2)}) %collective-permute-start.35) | collective-permute-done | bytes 196640 | tf_op jit(solution)/shard_map/ppermute | solution.py:40
  233.7 2.4 collective-permute-start.36
  236.1 4.8 %collective-permute-start.37 = (bf16[48,2048]{1,0:T(8,128)(2,1)S(1)}, bf16[48,2048]{1,0:T(8,128)(2,1)S(1)}, u32[]{:S(2)}, u32[]{:S(2)}) collective-permute-start(bf16[48,2048]{1,0:T(8,128)(2,1)S(1)} %shard_map.217.refs_0_), channel_id=1, source_target_pairs={{0,4},{1,5},{2,6},{3,7},{4,0},{5,1},{6,2},{7,3},{8,12},{9,13},{10,... | collective-permute-start | bytes 589832 | tf_op jit(solution)/shard_map/ppermute | solution.py:40
  240.9 2.3 collective-permute-start.38
  243.3 4.4 %collective-permute-done.37.refs_2_ = bf16[48,2048]{1,0:T(8,128)(2,1)S(1)} collective-permute-done((bf16[48,2048]{1,0:T(8,128)(2,1)S(1)}, bf16[48,2048]{1,0:T(8,128)(2,1)S(1)}, u32[]{:S(2)}, u32[]{:S(2)}) %collective-permute-start.37) | collective-permute-done | bytes 196640 | tf_op jit(solution)/shard_map/ppermute | solution.py:40
  247.7 5.1 %collective-permute-done.38.refs_3_ = bf16[48,2048]{1,0:T(8,128)(2,1)S(1)} collective-permute-done((bf16[48,2048]{1,0:T(8,128)(2,1)S(1)}, bf16[48,2048]{1,0:T(8,128)(2,1)S(1)}, u32[]{:S(2)}, u32[]{:S(2)}) %collective-permute-start.38) | collective-permute-done | bytes 196640 | tf_op jit(solution)/shard_map/ppermute | solution.py:40
  253.4 2.4 collective-permute-start.39
  255.8 1.4 place_own.1.held_ref
  257.7 1.4 place_other.1
  (78 shorter events, 12.3 us)
Async XLA Ops:
  1.4 16.9 %collective-permute-start = (bf16[64,1664]{1,0:T(8,128)(2,1)S(1)}, bf16[64,1664]{1,0:T(8,128)(2,1)S(1)}, u32[]{:S(2)}, u32[]{:S(2)}) collective-permute-start(bf16[64,1664]{1,0:T(8,128)(2,1)S(1)} %get-tuple-element.23.refs_0_), channel_id=1, source_target_pairs={{0,32},{8,40},{16,48},{24,56},{32,64},{40,72},{48,80},{56,88},{64,... | collective-permute-start | bytes 638984 | tf_op jit(solution)/shard_map/ppermute | solution.py:32
  5.8 14.4 %collective-permute-start.1 = (bf16[64,1664]{1,0:T(8,128)(2,1)S(1)}, bf16[64,1664]{1,0:T(8,128)(2,1)S(1)}, u32[]{:S(2)}, u32[]{:S(2)}) collective-permute-start(bf16[64,1664]{1,0:T(8,128)(2,1)S(1)} %get-tuple-element.23.refs_0_), channel_id=1, source_target_pairs={{0,480},{8,488},{16,496},{24,504},{32,0},{40,8},{48,16},{56,24},{6... | collective-permute-start | bytes 638984 | tf_op jit(solution)/shard_map/ppermute | solution.py:32
  18.3 8.7 %collective-permute-start.2 = (bf16[64,1664]{1,0:T(8,128)(2,1)S(1)}, bf16[64,1664]{1,0:T(8,128)(2,1)S(1)}, u32[]{:S(2)}, u32[]{:S(2)}) collective-permute-start(bf16[64,1664]{1,0:T(8,128)(2,1)S(1)} %collective-permute-done.refs_1_), channel_id=1, source_target_pairs={{0,32},{8,40},{16,48},{24,56},{32,64},{40,72},{48,80},{56,88},{64,... | collective-permute-start | bytes 638984 | tf_op jit(solution)/shard_map/ppermute | solution.py:32
  20.2 8.6 %collective-permute-start.3 = (bf16[64,1664]{1,0:T(8,128)(2,1)S(1)}, bf16[64,1664]{1,0:T(8,128)(2,1)S(1)}, u32[]{:S(2)}, u32[]{:S(2)}) collective-permute-start(bf16[64,1664]{1,0:T(8,128)(2,1)S(1)} %collective-permute-done.1.refs_2_), channel_id=1, source_target_pairs={{0,480},{8,488},{16,496},{24,504},{32,0},{40,8},{48,16},{56,24},{6... | collective-permute-start | bytes 638984 | tf_op jit(solution)/shard_map/ppermute | solution.py:32
  26.9 7.8 %collective-permute-start.4 = (bf16[64,1664]{1,0:T(8,128)(2,1)S(1)}, bf16[64,1664]{1,0:T(8,128)(2,1)S(1)}, u32[]{:S(2)}, u32[]{:S(2)}) collective-permute-start(bf16[64,1664]{1,0:T(8,128)(2,1)S(1)} %collective-permute-done.2.refs_3_), channel_id=1, source_target_pairs={{0,32},{8,40},{16,48},{24,56},{32,64},{40,72},{48,80},{56,88},{64,... | collective-permute-start | bytes 638984 | tf_op jit(solution)/shard_map/ppermute | solution.py:32
  28.9 7.8 %collective-permute-start.5 = (bf16[64,1664]{1,0:T(8,128)(2,1)S(1)}, bf16[64,1664]{1,0:T(8,128)(2,1)S(1)}, u32[]{:S(2)}, u32[]{:S(2)}) collective-permute-start(bf16[64,1664]{1,0:T(8,128)(2,1)S(1)} %collective-permute-done.3.refs_4_), channel_id=1, source_target_pairs={{0,480},{8,488},{16,496},{24,504},{32,0},{40,8},{48,16},{56,24},{6... | collective-permute-start | bytes 638984 | tf_op jit(solution)/shard_map/ppermute | solution.py:32
  34.7 7.8 %collective-permute-start.6 = (bf16[64,1664]{1,0:T(8,128)(2,1)S(1)}, bf16[64,1664]{1,0:T(8,128)(2,1)S(1)}, u32[]{:S(2)}, u32[]{:S(2)}) collective-permute-start(bf16[64,1664]{1,0:T(8,128)(2,1)S(1)} %collective-permute-done.4.refs_5_), channel_id=1, source_target_pairs={{0,32},{8,40},{16,48},{24,56},{32,64},{40,72},{48,80},{56,88},{64,... | collective-permute-start | bytes 638984 | tf_op jit(solution)/shard_map/ppermute | solution.py:32
  43.6 0.8 copy-start.3
  44.4 41.7 %collective-permute-start.7 = (bf16[512,1152]{1,0:T(8,128)(2,1)}, bf16[512,1152]{1,0:T(8,128)(2,1)S(1)}, u32[]{:S(2)}, u32[]{:S(2)}) collective-permute-start(bf16[512,1152]{1,0:T(8,128)(2,1)} %get-tuple-element.24.w0_ref), channel_id=1, source_target_pairs={{0,8},{8,0},{16,24},{24,16},{32,40},{40,32},{48,56},{56,48},{64,72... | collective-permute-start | bytes 3538952 | tf_op jit(solution)/shard_map/ppermute | solution.py:36
  47.6 41.6 %collective-permute-start.9 = (bf16[512,1152]{1,0:T(8,128)(2,1)}, bf16[512,1152]{1,0:T(8,128)(2,1)S(1)}, u32[]{:S(2)}, u32[]{:S(2)}) collective-permute-start(bf16[512,1152]{1,0:T(8,128)(2,1)} %get-tuple-element.24.w0_ref), channel_id=1, source_target_pairs={{0,24},{8,16},{16,8},{24,0},{32,56},{40,48},{48,40},{56,32},{64,88... | collective-permute-start | bytes 3538952 | tf_op jit(solution)/shard_map/ppermute | solution.py:36
  51.5 22.4 %collective-permute-start.22 = (bf16[64,1536]{1,0:T(8,128)(2,1)S(1)}, bf16[64,1536]{1,0:T(8,128)(2,1)S(1)}, u32[]{:S(2)}, u32[]{:S(2)}) collective-permute-start(bf16[64,1536]{1,0:T(8,128)(2,1)S(1)} %get-tuple-element.34.refs_0_), channel_id=1, source_target_pairs={{0,8},{8,0},{16,24},{24,16},{32,40},{40,32},{48,56},{56,48},{64,72... | collective-permute-start | bytes 589832 | tf_op jit(solution)/shard_map/ppermute | solution.py:36
  53.8 26.5 %collective-permute-start.23 = (bf16[64,1536]{1,0:T(8,128)(2,1)S(1)}, bf16[64,1536]{1,0:T(8,128)(2,1)S(1)}, u32[]{:S(2)}, u32[]{:S(2)}) collective-permute-start(bf16[64,1536]{1,0:T(8,128)(2,1)S(1)} %get-tuple-element.34.refs_0_), channel_id=1, source_target_pairs={{0,16},{8,24},{16,0},{24,8},{32,48},{40,56},{48,32},{56,40},{64,80... | collective-permute-start | bytes 589832 | tf_op jit(solution)/shard_map/ppermute | solution.py:36
  57.2 23.7 %collective-permute-start.24 = (bf16[64,1536]{1,0:T(8,128)(2,1)S(1)}, bf16[64,1536]{1,0:T(8,128)(2,1)S(1)}, u32[]{:S(2)}, u32[]{:S(2)}) collective-permute-start(bf16[64,1536]{1,0:T(8,128)(2,1)S(1)} %get-tuple-element.34.refs_0_), channel_id=1, source_target_pairs={{0,24},{8,16},{16,8},{24,0},{32,56},{40,48},{48,40},{56,32},{64,88... | collective-permute-start | bytes 589832 | tf_op jit(solution)/shard_map/ppermute | solution.py:36
  80.2 0.7 copy-start.5
  80.9 0.7 copy-start.7
  81.6 0.9 copy-start.6
  82.5 0.9 copy-start.8
  84.1 17.4 %copy-start = (bf16[384,2048]{1,0:T(8,128)(2,1)S(1)}, bf16[384,2048]{1,0:T(8,128)(2,1)}, u32[]{:S(2)}) copy-start(bf16[384,2048]{1,0:T(8,128)(2,1)} %x_ref.1) | copy-start | bytes 4718596
  84.1 17.4 %copy-start.9 = (f32[2048]{0:T(1024)S(1)}, f32[2048]{0:T(1024)}, u32[]{:S(2)}) copy-start(f32[2048]{0:T(1024)} %param.23) | copy-start | bytes 24580
  84.1 15.5 %collective-permute-start.25 = (bf16[256,1536]{1,0:T(8,128)(2,1)S(1)}, bf16[256,1536]{1,0:T(8,128)(2,1)S(1)}, u32[]{:S(2)}, u32[]{:S(2)}) collective-permute-start(bf16[256,1536]{1,0:T(8,128)(2,1)S(1)} %shard_map.214.refs_4_), channel_id=1, source_target_pairs={{0,32},{8,40},{16,48},{24,56},{32,64},{40,72},{48,80},{56,88},{64,... | collective-permute-start | bytes 2359304 | tf_op jit(solution)/shard_map/ppermute | solution.py:32
  86.2 18.1 %collective-permute-start.8 = (bf16[256,1152]{1,0:T(8,128)(2,1)S(1)}, bf16[256,1152]{1,0:T(8,128)(2,1)S(1)}, u32[]{:S(2)}, u32[]{:S(2)}) collective-permute-start(bf16[256,1152]{1,0:T(8,128)(2,1)S(1)} %slice.8), channel_id=1, source_target_pairs={{0,24},{8,16},{16,8},{24,0},{32,56},{40,48},{48,40},{56,32},{64,88... | collective-permute-start | bytes 1769480 | tf_op jit(solution)/shard_map/ppermute | solution.py:36
  89.3 15.1 %collective-permute-start.10 = (bf16[256,1152]{1,0:T(8,128)(2,1)S(1)}, bf16[256,1152]{1,0:T(8,128)(2,1)S(1)}, u32[]{:S(2)}, u32[]{:S(2)}) collective-permute-start(bf16[256,1152]{1,0:T(8,128)(2,1)S(1)} %slice.9), channel_id=1, source_target_pairs={{0,8},{8,0},{16,24},{24,16},{32,40},{40,32},{48,56},{56,48},{64,72... | collective-permute-start | bytes 1769480 | tf_op jit(solution)/shard_map/ppermute | solution.py:36
  91.2 32.6 %collective-permute-start.26 = (bf16[256,1536]{1,0:T(8,128)(2,1)S(1)}, bf16[256,1536]{1,0:T(8,128)(2,1)}, u32[]{:S(2)}, u32[]{:S(2)}) collective-permute-start(bf16[256,1536]{1,0:T(8,128)(2,1)S(1)} %shard_map.214.refs_4_), channel_id=1, source_target_pairs={{0,480},{8,488},{16,496},{24,504},{32,0},{40,8},{48,16},{56,24},{6... | collective-permute-start | bytes 2359304 | tf_op jit(solution)/shard_map/ppermute | solution.py:32
  99.6 4.8 %copy-start.1 = (bf16[256,1536]{1,0:T(8,128)(2,1)}, bf16[256,1536]{1,0:T(8,128)(2,1)S(1)}, u32[]{:S(2)}) copy-start(bf16[256,1536]{1,0:T(8,128)(2,1)S(1)} %collective-permute-done.25.refs_5_) | copy-start | bytes 2359300
  99.6 29.1 %collective-permute-start.27 = (bf16[256,1536]{1,0:T(8,128)(2,1)S(1)}, bf16[256,1536]{1,0:T(8,128)(2,1)}, u32[]{:S(2)}, u32[]{:S(2)}) collective-permute-start(bf16[256,1536]{1,0:T(8,128)(2,1)S(1)} %collective-permute-done.25.refs_5_), channel_id=1, source_target_pairs={{0,32},{8,40},{16,48},{24,56},{32,64},{40,72},{48,80},{56,88},{64,... | collective-permute-start | bytes 2359304 | tf_op jit(solution)/shard_map/ppermute | solution.py:32
  101.5 2.9 %copy-start.12 = (f32[384,1]{0,1:T(1,128)S(1)}, f32[384,1]{0,1:T(1,128)}, u32[]{:S(2)}) copy-start(f32[384,1]{0,1:T(1,128)} %param.31) | copy-start | bytes 4612
  101.5 2.9 %copy-start.13 = (f32[256]{0:T(256)S(1)}, f32[256]{0:T(256)}, u32[]{:S(2)}) copy-start(f32[256]{0:T(256)} %param.33) | copy-start | bytes 3076
  101.6 2.9 %copy-start.14 = (f32[256]{0:T(256)S(1)}, f32[256]{0:T(256)}, u32[]{:S(2)}) copy-start(f32[256]{0:T(256)} %param.35) | copy-start | bytes 3076
  101.6 2.9 %copy-start.15 = (f32[256]{0:T(256)S(1)}, f32[256]{0:T(256)}, u32[]{:S(2)}) copy-start(f32[256]{0:T(256)} %param.36) | copy-start | bytes 3076
  101.6 2.9 %copy-start.16 = (f32[128]{0:T(128)S(1)}, f32[128]{0:T(128)}, u32[]{:S(2)}) copy-start(f32[128]{0:T(128)} %param.25) | copy-start | bytes 1540
  101.6 2.8 %copy-start.17 = (f32[128]{0:T(128)S(1)}, f32[128]{0:T(128)}, u32[]{:S(2)}) copy-start(f32[128]{0:T(128)} %param.27) | copy-start | bytes 1540
  101.6 2.8 %copy-start.18 = (f32[128]{0:T(128)S(1)}, f32[128]{0:T(128)}, u32[]{:S(2)}) copy-start(f32[128]{0:T(128)} %param.29) | copy-start | bytes 1540
  101.6 2.8 %copy-start.19 = (f32[128]{0:T(128)S(1)}, f32[128]{0:T(128)}, u32[]{:S(2)}) copy-start(f32[128]{0:T(128)} %param.30) | copy-start | bytes 1540
  112.7 39.5 %copy-start.10 = (f32[2048]{0:T(1024)S(1)}, f32[2048]{0:T(1024)}, u32[]{:S(2)}) copy-start(f32[2048]{0:T(1024)} %param.39) | copy-start | bytes 24580
  112.7 17.9 %collective-permute-start.11 = (bf16[192,2048]{1,0:T(8,128)(2,1)S(1)}, bf16[192,2048]{1,0:T(8,128)(2,1)S(1)}, u32[]{:S(2)}, u32[]{:S(2)}) collective-permute-start(bf16[192,2048]{1,0:T(8,128)(2,1)S(1)} %get-tuple-element.26), channel_id=1, source_target_pairs={{0,1},{1,0},{2,3},{3,2},{4,5},{5,4},{6,7},{7,6},{8,9},{9,8},{10,11... | collective-permute-start | bytes 2359304 | tf_op jit(solution)/shard_map/ppermute | solution.py:44
  123.8 36.7 %collective-permute-start.28 = (bf16[256,1536]{1,0:T(8,128)(2,1)}, bf16[256,1536]{1,0:T(8,128)(2,1)S(1)}, u32[]{:S(2)}, u32[]{:S(2)}) collective-permute-start(bf16[256,1536]{1,0:T(8,128)(2,1)} %collective-permute-done.26.refs_6_), channel_id=1, source_target_pairs={{0,480},{8,488},{16,496},{24,504},{32,0},{40,8},{48,16},{56,24},{6... | collective-permute-start | bytes 2359304 | tf_op jit(solution)/shard_map/ppermute | solution.py:32
  128.7 34.1 %collective-permute-start.29 = (bf16[256,1536]{1,0:T(8,128)(2,1)}, bf16[256,1536]{1,0:T(8,128)(2,1)S(1)}, u32[]{:S(2)}, u32[]{:S(2)}) collective-permute-start(bf16[256,1536]{1,0:T(8,128)(2,1)} %collective-permute-done.27.refs_7_), channel_id=1, source_target_pairs={{0,32},{8,40},{16,48},{24,56},{32,64},{40,72},{48,80},{56,88},{64,... | collective-permute-start | bytes 2359304 | tf_op jit(solution)/shard_map/ppermute | solution.py:32
  132.0 0.7 copy-start.20
  132.7 0.7 copy-start.21
  133.3 71.2 %copy-start.2 = (bf16[256,1536]{1,0:T(8,128)(2,1)S(1)}, bf16[256,1536]{1,0:T(8,128)(2,1)}, u32[]{:S(2)}) copy-start(bf16[256,1536]{1,0:T(8,128)(2,1)} %copy-done.1) | copy-start | bytes 2359300
  133.3 71.3 %copy-start.11 = (f32[1024]{0:T(1024)S(1)}, f32[1024]{0:T(1024)}, u32[]{:S(2)}) copy-start(f32[1024]{0:T(1024)} %param.41) | copy-start | bytes 12292
  133.3 9.7 %collective-permute-start.12 = (bf16[48,2048]{1,0:T(8,128)(2,1)}, bf16[48,2048]{1,0:T(8,128)(2,1)S(1)}, u32[]{:S(2)}, u32[]{:S(2)}) collective-permute-start(bf16[48,2048]{1,0:T(8,128)(2,1)} %get-tuple-element.28), channel_id=1, source_target_pairs={{0,2},{1,3},{2,0},{3,1},{4,6},{5,7},{6,4},{7,5},{8,10},{9,11},{10,... | collective-permute-start | bytes 589832 | tf_op jit(solution)/shard_map/ppermute | solution.py:40
  136.6 38.8 %copy-start.4 = (bf16[512,512]{1,0:T(8,128)(2,1)S(1)}, bf16[512,512]{1,0:T(8,128)(2,1)}, u32[]{:S(2)}) copy-start(bf16[512,512]{1,0:T(8,128)(2,1)} %copy-done.3) | copy-start | bytes 1572868
  136.6 44.3 %collective-permute-start.19 = (bf16[512,512]{1,0:T(8,128)(2,1)}, bf16[512,512]{1,0:T(8,128)(2,1)S(1)}, u32[]{:S(2)}, u32[]{:S(2)}) collective-permute-start(bf16[512,512]{1,0:T(8,128)(2,1)} %copy-done.3), channel_id=1, source_target_pairs={{0,8},{8,0},{16,24},{24,16},{32,40},{40,32},{48,56},{56,48},{64,72... | collective-permute-start | bytes 1572872 | tf_op jit(solution)/shard_map/ppermute | solution.py:36
  138.7 9.5 %collective-permute-start.13 = (bf16[48,2048]{1,0:T(8,128)(2,1)}, bf16[48,2048]{1,0:T(8,128)(2,1)S(1)}, u32[]{:S(2)}, u32[]{:S(2)}) collective-permute-start(bf16[48,2048]{1,0:T(8,128)(2,1)} %copy-done.21), channel_id=1, source_target_pairs={{0,4},{1,5},{2,6},{3,7},{4,0},{5,1},{6,2},{7,3},{8,12},{9,13},{10,... | collective-permute-start | bytes 589832 | tf_op jit(solution)/shard_map/ppermute | solution.py:40
  143.0 9.2 %collective-permute-start.14 = (bf16[48,2048]{1,0:T(8,128)(2,1)}, bf16[48,2048]{1,0:T(8,128)(2,1)S(1)}, u32[]{:S(2)}, u32[]{:S(2)}) collective-permute-start(bf16[48,2048]{1,0:T(8,128)(2,1)} %copy-done.20), channel_id=1, source_target_pairs={{0,6},{1,7},{2,4},{3,5},{4,2},{5,3},{6,0},{7,1},{8,14},{9,15},{10,... | collective-permute-start | bytes 589832 | tf_op jit(solution)/shard_map/ppermute | solution.py:40
  153.1 14.2 %collective-permute-start.15 = (bf16[48,2048]{1,0:T(8,128)(2,1)S(1)}, bf16[48,2048]{1,0:T(8,128)(2,1)S(1)}, u32[]{:S(2)}, u32[]{:S(2)}) collective-permute-start(bf16[48,2048]{1,0:T(8,128)(2,1)S(1)} %get-tuple-element.32.refs_0_), channel_id=1, source_target_pairs={{0,2},{1,3},{2,0},{3,1},{4,6},{5,7},{6,4},{7,5},{8,10},{9,11},{10,... | collective-permute-start | bytes 589832 | tf_op jit(solution)/shard_map/ppermute | solution.py:40
  156.4 12.9 %collective-permute-start.16 = (bf16[48,2048]{1,0:T(8,128)(2,1)S(1)}, bf16[48,2048]{1,0:T(8,128)(2,1)S(1)}, u32[]{:S(2)}, u32[]{:S(2)}) collective-permute-start(bf16[48,2048]{1,0:T(8,128)(2,1)S(1)} %get-tuple-element.32.refs_0_), channel_id=1, source_target_pairs={{0,4},{1,5},{2,6},{3,7},{4,0},{5,1},{6,2},{7,3},{8,12},{9,13},{10,... | collective-permute-start | bytes 589832 | tf_op jit(solution)/shard_map/ppermute | solution.py:40
  160.5 11.8 %collective-permute-start.17 = (bf16[48,2048]{1,0:T(8,128)(2,1)S(1)}, bf16[48,2048]{1,0:T(8,128)(2,1)S(1)}, u32[]{:S(2)}, u32[]{:S(2)}) collective-permute-start(bf16[48,2048]{1,0:T(8,128)(2,1)S(1)} %get-tuple-element.32.refs_0_), channel_id=1, source_target_pairs={{0,6},{1,7},{2,4},{3,5},{4,2},{5,3},{6,0},{7,1},{8,14},{9,15},{10,... | collective-permute-start | bytes 589832 | tf_op jit(solution)/shard_map/ppermute | solution.py:40
  162.8 41.8 %collective-permute-start.30 = (bf16[256,1536]{1,0:T(8,128)(2,1)S(1)}, bf16[256,1536]{1,0:T(8,128)(2,1)S(1)}, u32[]{:S(2)}, u32[]{:S(2)}) collective-permute-start(bf16[256,1536]{1,0:T(8,128)(2,1)S(1)} %collective-permute-done.28.refs_8_), channel_id=1, source_target_pairs={{0,480},{8,488},{16,496},{24,504},{32,0},{40,8},{48,16},{56,24},{6... | collective-permute-start | bytes 2359304 | tf_op jit(solution)/shard_map/ppermute | solution.py:32
  167.3 37.2 %collective-permute-start.31 = (bf16[256,1536]{1,0:T(8,128)(2,1)S(1)}, bf16[256,1536]{1,0:T(8,128)(2,1)S(1)}, u32[]{:S(2)}, u32[]{:S(2)}) collective-permute-start(bf16[256,1536]{1,0:T(8,128)(2,1)S(1)} %collective-permute-done.29.refs_9_), channel_id=1, source_target_pairs={{0,32},{8,40},{16,48},{24,56},{32,64},{40,72},{48,80},{56,88},{64,... | collective-permute-start | bytes 2359304 | tf_op jit(solution)/shard_map/ppermute | solution.py:32
  172.9 31.6 %collective-permute-start.18 = (bf16[192,2048]{1,0:T(8,128)(2,1)S(1)}, bf16[192,2048]{1,0:T(8,128)(2,1)S(1)}, u32[]{:S(2)}, u32[]{:S(2)}) collective-permute-start(bf16[192,2048]{1,0:T(8,128)(2,1)S(1)} %shard_map.213.own_ref), channel_id=1, source_target_pairs={{0,1},{1,0},{2,3},{3,2},{4,5},{5,4},{6,7},{7,6},{8,9},{9,8},{10,11... | collective-permute-start | bytes 2359304 | tf_op jit(solution)/shard_map/ppermute | solution.py:44
  175.4 17.8 %collective-permute-start.20 = (bf16[512,512]{1,0:T(8,128)(2,1)S(1)}, bf16[512,512]{1,0:T(8,128)(2,1)S(1)}, u32[]{:S(2)}, u32[]{:S(2)}) collective-permute-start(bf16[512,512]{1,0:T(8,128)(2,1)S(1)} %copy-done.4), channel_id=1, source_target_pairs={{0,16},{8,24},{16,0},{24,8},{32,48},{40,56},{48,32},{56,40},{64,80... | collective-permute-start | bytes 1572872 | tf_op jit(solution)/shard_map/ppermute | solution.py:36
  180.9 23.6 %collective-permute-start.21 = (bf16[512,512]{1,0:T(8,128)(2,1)S(1)}, bf16[512,512]{1,0:T(8,128)(2,1)S(1)}, u32[]{:S(2)}, u32[]{:S(2)}) collective-permute-start(bf16[512,512]{1,0:T(8,128)(2,1)S(1)} %copy-done.4), channel_id=1, source_target_pairs={{0,24},{8,16},{16,8},{24,0},{32,56},{40,48},{48,40},{56,32},{64,88... | collective-permute-start | bytes 1572872 | tf_op jit(solution)/shard_map/ppermute | solution.py:36
  210.7 4.3 %collective-permute-start.32 = (bf16[192,2048]{1,0:T(8,128)(2,1)S(1)}, bf16[192,2048]{1,0:T(8,128)(2,1)S(1)}, u32[]{:S(2)}, u32[]{:S(2)}) collective-permute-start(bf16[192,2048]{1,0:T(8,128)(2,1)S(1)} %get-tuple-element.36), channel_id=1, source_target_pairs={{0,1},{1,0},{2,3},{3,2},{4,5},{5,4},{6,7},{7,6},{8,9},{9,8},{10,11... | collective-permute-start | bytes 2359304 | tf_op jit(solution)/shard_map/ppermute | solution.py:44
  215.7 9.6 %collective-permute-start.33 = (bf16[48,2048]{1,0:T(8,128)(2,1)S(1)}, bf16[48,2048]{1,0:T(8,128)(2,1)S(1)}, u32[]{:S(2)}, u32[]{:S(2)}) collective-permute-start(bf16[48,2048]{1,0:T(8,128)(2,1)S(1)} %get-tuple-element.38), channel_id=1, source_target_pairs={{0,2},{1,3},{2,0},{3,1},{4,6},{5,7},{6,4},{7,5},{8,10},{9,11},{10,... | collective-permute-start | bytes 589832 | tf_op jit(solution)/shard_map/ppermute | solution.py:40
  217.9 10.3 %collective-permute-start.34 = (bf16[48,2048]{1,0:T(8,128)(2,1)S(1)}, bf16[48,2048]{1,0:T(8,128)(2,1)S(1)}, u32[]{:S(2)}, u32[]{:S(2)}) collective-permute-start(bf16[48,2048]{1,0:T(8,128)(2,1)S(1)} %get-tuple-element.39), channel_id=1, source_target_pairs={{0,4},{1,5},{2,6},{3,7},{4,0},{5,1},{6,2},{7,3},{8,12},{9,13},{10,... | collective-permute-start | bytes 589832 | tf_op jit(solution)/shard_map/ppermute | solution.py:40
  221.1 11.8 %collective-permute-start.35 = (bf16[48,2048]{1,0:T(8,128)(2,1)S(1)}, bf16[48,2048]{1,0:T(8,128)(2,1)S(1)}, u32[]{:S(2)}, u32[]{:S(2)}) collective-permute-start(bf16[48,2048]{1,0:T(8,128)(2,1)S(1)} %get-tuple-element.40), channel_id=1, source_target_pairs={{0,6},{1,7},{2,4},{3,5},{4,2},{5,3},{6,0},{7,1},{8,14},{9,15},{10,... | collective-permute-start | bytes 589832 | tf_op jit(solution)/shard_map/ppermute | solution.py:40
  233.7 9.6 %collective-permute-start.36 = (bf16[48,2048]{1,0:T(8,128)(2,1)S(1)}, bf16[48,2048]{1,0:T(8,128)(2,1)S(1)}, u32[]{:S(2)}, u32[]{:S(2)}) collective-permute-start(bf16[48,2048]{1,0:T(8,128)(2,1)S(1)} %shard_map.217.refs_0_), channel_id=1, source_target_pairs={{0,2},{1,3},{2,0},{3,1},{4,6},{5,7},{6,4},{7,5},{8,10},{9,11},{10,... | collective-permute-start | bytes 589832 | tf_op jit(solution)/shard_map/ppermute | solution.py:40
  236.1 11.6 %collective-permute-start.37 = (bf16[48,2048]{1,0:T(8,128)(2,1)S(1)}, bf16[48,2048]{1,0:T(8,128)(2,1)S(1)}, u32[]{:S(2)}, u32[]{:S(2)}) collective-permute-start(bf16[48,2048]{1,0:T(8,128)(2,1)S(1)} %shard_map.217.refs_0_), channel_id=1, source_target_pairs={{0,4},{1,5},{2,6},{3,7},{4,0},{5,1},{6,2},{7,3},{8,12},{9,13},{10,... | collective-permute-start | bytes 589832 | tf_op jit(solution)/shard_map/ppermute | solution.py:40
  240.9 11.8 %collective-permute-start.38 = (bf16[48,2048]{1,0:T(8,128)(2,1)S(1)}, bf16[48,2048]{1,0:T(8,128)(2,1)S(1)}, u32[]{:S(2)}, u32[]{:S(2)}) collective-permute-start(bf16[48,2048]{1,0:T(8,128)(2,1)S(1)} %shard_map.217.refs_0_), channel_id=1, source_target_pairs={{0,6},{1,7},{2,4},{3,5},{4,2},{5,3},{6,0},{7,1},{8,14},{9,15},{10,... | collective-permute-start | bytes 589832 | tf_op jit(solution)/shard_map/ppermute | solution.py:40
  253.4 4.3 %collective-permute-start.39 = (bf16[192,2048]{1,0:T(8,128)(2,1)S(1)}, bf16[192,2048]{1,0:T(8,128)(2,1)S(1)}, u32[]{:S(2)}, u32[]{:S(2)}) collective-permute-start(bf16[192,2048]{1,0:T(8,128)(2,1)S(1)} %shard_map.218.own_ref), channel_id=1, source_target_pairs={{0,1},{1,0},{2,3},{3,2},{4,5},{5,4},{6,7},{7,6},{8,9},{9,8},{10,11... | collective-permute-start | bytes 2359304 | tf_op jit(solution)/shard_map/ppermute | solution.py:44
where the time goes:
time: 261 us; the launch traced here: 259 us
  starting transfers between devices  140 us (54%)
  waiting for transfers between devices  83.7 us (32%)
  Pallas kernels  27.8 us (11%)
  local copies, waits for them, and re-layouts  6.5 us (2%)
    ppermute x14, starting transfers between devices, z_send(): return lax.ppermute(value, ZY, z_pairs(step))  50.5 us
    ppermute x10, waiting for transfers between devices, y_send(): return lax.ppermute(value, ZY, y_pairs(mask))  39.9 us
    ppermute x12, starting transfers between devices, x_send(): return lax.ppermute(value, 'tp', [(t, t ^ 2 * mask) for t in range(8)])  39.4 us
    ppermute x10, starting transfers between devices, y_send(): return lax.ppermute(value, ZY, y_pairs(mask))  31.9 us
    ppermute x12, waiting for transfers between devices, x_send(): return lax.ppermute(value, 'tp', [(t, t ^ 2 * mask) for t in range(8)])  25.4 us
    pallas_call x11, Pallas kernels, call(): pl.pallas_call(kernel, out_shape=[pltpu.VMEM(s, t) for s, t in outs], in_...  23.6 us
    ppermute x4, starting transfers between devices, core_swap(): return lax.ppermute(value, 'tp', [(t, t ^ 1) for t in range(8)])  18.3 us
    ppermute x14, waiting for transfers between devices, z_send(): return lax.ppermute(value, ZY, z_pairs(step))  16.1 us
  transfers between devices with their start and end apart: 40, of which 18 were waited for; matrix products, arithmetic and copies ran while one was open for 0% of the time, Pallas kernels for 6%

commit v1 on v0

--- a/solution.py
+++ b/solution.py
@@ -16,8 +16,7 @@
 OFFSETS = (0, -1, 1, -2, 2, -3, 3, 4)
 LEVELS = (32, 16, 8, 4, 2, 1)
 ZY = ("rep", "fs")
-EXTRA = 512
-VMEM_LIMIT = 10 * 1024 * 1024
+VMEM_LIMIT = 12 * 1024 * 1024
 
 
 def z_pairs(step):
@@ -36,22 +35,36 @@
     return lax.ppermute(value, ZY, y_pairs(mask))
 
 
-def x_send(value, mask):
-    return lax.ppermute(value, "tp", [(t, t ^ (2 * mask)) for t in range(8)])
-
-
 def core_swap(value):
     return lax.ppermute(value, "tp", [(t, t ^ 1) for t in range(8)])
 
 
-def z_gather(own, far_step):
+X_GROUPS = [[0, 2, 4, 6], [1, 3, 5, 7]]
+
+
+def x_exchange(pieces):
+    return lax.all_to_all(pieces, "tp", 0, 0, axis_index_groups=X_GROUPS, tiled=True)
+
+
+def z_mixed(own):
+    got = {0: own}
+    for k in (1, 2):
+        got[-k] = z_send(own, k)
+        got[k] = z_send(own, -k)
+    got[-3] = z_send(got[-2], 1)
+    got[3] = z_send(got[2], -1)
+    got[4] = z_send(got[-2], 2)
+    return [got[d] for d in OFFSETS]
+
+
+def z_relay(own):
     up, down = own, own
     got = {0: own}
     for k in range(1, 4):
         up = z_send(up, 1)
         down = z_send(down, -1)
         got[-k], got[k] = up, down
-    got[4] = z_send(up if far_step > 0 else down, far_step)
+    got[4] = z_send(up, 1)
     return [got[d] for d in OFFSETS]
 
 
@@ -59,12 +72,17 @@
     first = y_send(own, 1)
     third = y_send(own, 3)
     cut = own.shape[0] // 2
-    return (own, first, y_send(first[:cut], 3), y_send(third[cut:], 1), third)
-
-
-def y_direct(own):
-    far = y_send(own, 2)
-    return own, y_send(own, 1), far, y_send(own, 3)
+    return (
+        (own, first, third),
+        (y_send(first[:cut], 3), y_send(third[cut:], 1)),
+    )
+
+
+Y_GROUPS = [[4 * z + y for y in range(4)] for z in range(8)]
+
+
+def y_exchange(pieces):
+    return lax.all_to_all(pieces, "fs", 0, 0, axis_index_groups=Y_GROUPS, tiled=True)
 
 
 def low_lanes(rows):
@@ -131,40 +149,20 @@
         at += held[n].shape[1]
     copies[5].wait()
     copies[8].wait()
-    attention[:, at:1152] = (held[5][...] * column(held[8])).astype(BF)
+    attention[:, at:] = (held[5][...] * column(held[8])).astype(BF)
     copies[7].wait()
     copies[9].wait()
     low = (held[7][...] * column(held[9])).astype(BF)
-    attention[:, 1152:] = low[:, :EXTRA]
-    ffn[:, 1024:] = low[:, EXTRA:]
     copies[6].wait()
-    ffn[:, :1024] = held[6][...].astype(BF)
+    up = held[6][...].astype(BF)
+    for s in range(4):
+        ffn[s, :, :1024] = up
+        ffn[s, :, 1024:] = low
 
 
 def stack_kernel(*refs):
-    blocks, (tables_ref, low_ref) = refs[:8], refs[8:]
-    for n, ref in enumerate(blocks):
-        at = slice(64 * n, 64 * (n + 1))
-        tables_ref[at, :] = ref[:, :1152]
-        low_ref[at, :] = ref[:, 1152:]
-
-
-def rows_kernel(where_ref, *refs):
-    blocks, out_ref = refs[:4], refs[4]
-    for mask, ref in enumerate(blocks):
-        out_ref[pl.ds(pl.multiple_of((where_ref[1] ^ mask) * 64, 64), 64), :] = ref[...]
-
-
-def half_kernel(where_ref, *refs):
-    blocks, out_ref = refs[:4], refs[4]
-    for mask, ref in enumerate(blocks):
-        out_ref[pl.ds(pl.multiple_of((where_ref[3] ^ mask) * 48, 48), 48), :] = ref[...]
-
-
-def join_kernel(where_ref, keep_ref, got_ref, *outs):
-    for mask, ref in enumerate(outs):
-        at = pl.ds(pl.multiple_of((where_ref[3] ^ mask) * 48, 48), 48)
-        ref[...] = (keep_ref[at, :].astype(F32) + got_ref[at, :].astype(F32)).astype(BF)
+    for n, ref in enumerate(refs[:-1]):
+        refs[-1][64 * n : 64 * (n + 1), :] = ref[...]
 
 
 def norm_kernel(where_ref, x_ref, gain_ref, out_ref, keep_ref):
@@ -209,14 +207,28 @@
 TN = (((0,), (0,)), ((), ()))
 
 
+def early_kernel(x_ref, w0_ref, w1_ref, w3_ref, out_ref):
+    for lo in range(0, 896, 128):
+        total = None
+        for mask, ref in ((0, w0_ref), (1, w1_ref), (3, w3_ref)):
+            piece = jnp.dot(
+                x_ref[:, 512 * mask : 512 * (mask + 1)],
+                ref[:, lo : lo + 128],
+                preferred_element_type=F32,
+            )
+            total = piece if total is None else total + piece
+        out_ref[:, lo : lo + 128] = total
+
+
 def mixing_kernel(
     where_ref,
     x_ref,
+    early_ref,
     w0_ref,
     w1_ref,
+    w3_ref,
     w2a_ref,
     w2b_ref,
-    w3_ref,
     probe_scale,
     lookup_scale,
     forget_scale,
@@ -245,13 +257,11 @@
     )
 
     def project(lo, hi, scale):
-        total = None
-        for mask, start, size, ref in parts:
-            at = 512 * mask + start
-            piece = jnp.dot(
-                x_ref[:, at : at + size], ref[:, lo:hi], preferred_element_type=F32
+        total = early_ref[:, lo:hi]
+        for start, ref in ((1024, w2a_ref), (1280, w2b_ref)):
+            total = total + jnp.dot(
+                x_ref[:, start : start + 256], ref[:, lo:hi], preferred_element_type=F32
             )
-            total = piece if total is None else total + piece
         return total * scale[...]
 
     q_ref[...] = (silu(project(0, 128, probe_scale)) * 128**-0.5).astype(BF).astype(F32)
@@ -304,16 +314,15 @@
             ).astype(BF)
 
 
-def middle_kernel(where_ref, x_ref, gain_ref, *refs):
-    parts, (residual_ref, normed_ref) = refs[:4], refs[4:]
+def middle_kernel(where_ref, parts_ref, x_ref, gain_ref, residual_ref, normed_ref):
     z = where_ref[0]
     rows = 48
     mixed = []
     for k in range(16):
         at = slice(128 * k, 128 * (k + 1))
-        total = parts[0][:, at].astype(F32)
-        for part in parts[1:]:
-            total = total + part[:, at].astype(F32)
+        total = parts_ref[0, :, at].astype(F32)
+        for s in range(1, 4):
+            total = total + parts_ref[s, :, at].astype(F32)
         mixed.append(total)
     mixed = b_to_a(mixed, rows)
     own = to_a(lambda s: x_ref[:, pl.ds(s, 128)].astype(F32), z)
@@ -328,12 +337,19 @@
         square = square + jnp.sum(tile * tile, axis=-1, keepdims=True)
     factor = lax.rsqrt(square * (1.0 / D) + EPS)
     for k in range(16):
-        normed_ref[:, 128 * k : 128 * (k + 1)] = (kept[k] * factor * gain[k]).astype(BF)
-
-
-def ffn_kernel(where_ref, own_ref, other_ref, scale_ref, *refs):
-    lows, refs = refs[:4], refs[4:]
-    pieces, (keep_ref, send_ref, hidden_ref, part_ref) = refs[:8], refs[8:]
+        tile = (kept[k] * factor * gain[k]).astype(BF)
+        for s in range(4):
+            normed_ref[s, :, 128 * k : 128 * (k + 1)] = tile
+
+
+def join_kernel(mine_ref, got_ref, out_ref):
+    for s in range(4):
+        at = slice(48 * s, 48 * (s + 1))
+        out_ref[s] = (mine_ref[at, :].astype(F32) + got_ref[at, :].astype(F32)).astype(BF)
+
+
+def ffn_kernel(own_ref, other_ref, scale_ref, *refs):
+    pieces, (keep_ref, send_ref, hidden_ref) = refs[:8], refs[8:]
     for half, ref in ((0, own_ref), (1, other_ref)):
         for lo in range(0, 1024, 256):
             total = None
@@ -346,38 +362,24 @@
                 total = part if total is None else total + part
             value = jnp.maximum(total * scale_ref[:, lo : lo + 256], 0.0)
             hidden_ref[half, :, lo : lo + 256] = (value * value).astype(BF)
-    rows = ROWS // 2
-    low = low_lanes(rows)
     for half, ref in ((1, send_ref), (0, keep_ref)):
-        for y in range(4):
-            part_ref[where_ref[1] ^ y] = lax.dot_general(
-                hidden_ref[half, :, :EXTRA], lows[y][...], NT, preferred_element_type=F32
-            )
         for i, piece in enumerate(pieces):
-            total = lax.dot_general(
-                hidden_ref[half, :, EXTRA:], piece[:, 1024:], NT, preferred_element_type=F32
-            )
-            at = slice(128 * (i // 2), 128 * (i // 2 + 1))
-            for t in range(2):
-                even, odd = part_ref[2 * t, :, at], part_ref[2 * t + 1, :, at]
-                if i % 2 == 0:
-                    extra = jnp.where(low, even, turn(odd))
-                else:
-                    extra = jnp.where(low, turn(even), odd)
-                ref[:, 256 * i + 128 * t : 256 * i + 128 * (t + 1)] = (
-                    total[:, 128 * t : 128 * (t + 1)] + extra
-                ).astype(BF)
-
-
-def last_kernel(where_ref, residual_ref, *refs):
-    parts, out_ref = refs[:4], refs[4]
+            ref[:, 256 * i : 256 * (i + 1)] = lax.dot_general(
+                hidden_ref[half], piece[:, 1024:], NT, preferred_element_type=F32
+            ).astype(BF)
+
+
+def last_kernel(where_ref, parts_ref, residual_ref, out_ref):
+    z = where_ref[0]
     for i, d in enumerate(OFFSETS):
-        base = pl.multiple_of(((where_ref[0] + d) & 7) * 256, 256)
+        base = pl.multiple_of(((z + d) & 7) * 256, 256)
         at = slice(256 * i, 256 * (i + 1))
-        total = parts[0][:, at].astype(F32)
-        for part in parts[1:]:
-            total = total + part[:, at].astype(F32)
-        out_ref[:, pl.ds(base, 256)] = (residual_ref[:, at].astype(F32) + total).astype(BF)
+        total = parts_ref[0, :, at].astype(F32)
+        for s in range(1, 4):
+            total = total + parts_ref[s, :, at].astype(F32)
+        tile = (residual_ref[:, at].astype(F32) + total).astype(BF)
+        for s in range(4):
+            out_ref[s, :, pl.ds(base, 256)] = tile
 
 
 def place_own_kernel(where_ref, own_ref, out_ref, sem):
@@ -482,7 +484,7 @@
     far = pl.BlockSpec(memory_space=pl.ANY)
     attention, ffn = pl.pallas_call(
         cast_kernel,
-        out_shape=[pltpu.VMEM((64, 1152 + EXTRA), BF), pltpu.VMEM((64, 2048 - EXTRA), BF)],
+        out_shape=[pltpu.VMEM((64, 1152), BF), pltpu.VMEM((4, 64, 2048), BF)],
         in_specs=[far] * 10,
         out_specs=[vmem] * 2,
         scratch_shapes=[pltpu.VMEM(w.shape, F32) for w in tables]
@@ -492,20 +494,13 @@
     )(
         *(pltpu.with_memory_space_constraint(w, pltpu.HBM) for w in tables)
     )
-    along_z, low_z = call(
-        stack_kernel,
-        [((512, 1152), BF), ((512, EXTRA), BF)],
-        [],
-        *(near(b) for b in z_gather(attention, 1)),
-    )
-    tables = y_gather(along_z)
-    extra = y_direct(low_z)
-    (along_y,) = call(
-        rows_kernel, [((256, 2048 - EXTRA), BF)], [], where, *(near(b) for b in y_direct(ffn))
-    )
-    pieces = z_gather(along_y, 1)
+    (along_z,) = call(stack_kernel, [((512, 1152), BF)], [], *(near(b) for b in z_mixed(attention)))
+    first_tables, second_tables = y_gather(along_z)
+    pieces = z_relay(y_exchange(ffn).reshape(256, 2048))
 
     (normed,) = call(norm_kernel, [((ROWS, D), BF)], [((48, D), F32)], where, x, pre_gain[None, :])
+    first_tables = [near(t) for t in first_tables]
+    (early,) = call(early_kernel, [((ROWS, 896), F32)], [], near(normed), *first_tables)
     keep, send = call(
         mixing_kernel,
         [((ROWS // 2, D), BF)] * 2,
@@ -520,7 +515,9 @@
         ],
         where,
         near(normed),
-        *(near(t) for t in tables),
+        near(early),
+        *first_tables,
+        *(near(t) for t in second_tables),
         s_probe[None, :],
         s_lookup[None, :],
         s_forget[None, :],
@@ -531,45 +528,36 @@
         head_gain[None, :],
     )
 
-    piece = ((48, D), BF)
-
     def reduce_rows(keep, send):
-        own, *others = call(join_kernel, [piece] * 4, [], where, near(keep), near(core_swap(send)))
-        got = {m: x_send(others[m - 1], m) for m in (2, 1, 3)}
-        return near(own), near(got[1]), near(got[2]), near(got[3])
-
-    def spread_rows(own):
-        got = {m: x_send(own, m) for m in (2, 1, 3)}
-        (half,) = call(
-            half_kernel,
-            [((ROWS // 2, D), BF)],
-            [],
-            where,
-            near(own),
-            near(got[1]),
-            near(got[2]),
-            near(got[3]),
-        )
+        (both,) = call(join_kernel, [((4, 48, D), BF)], [], near(keep), near(core_swap(send)))
+        return near(x_exchange(both))
+
+    def spread_rows(copies):
+        half = x_exchange(copies).reshape(ROWS // 2, D)
         return half, core_swap(half)
 
     own_rows = lax.dynamic_slice_in_dim(x, where[2] * 192 + where[3] * 48, 48, 0)
     residual, normed_share = call(
-        middle_kernel, [piece] * 2, [], where, own_rows, mlp_gain[None, :], *reduce_rows(keep, send)
+        middle_kernel,
+        [((48, D), BF), ((4, 48, D), BF)],
+        [],
+        where,
+        reduce_rows(keep, send),
+        own_rows,
+        mlp_gain[None, :],
     )
     own, other = spread_rows(normed_share)
-    keep, send = call(
+    sums = call(
         ffn_kernel,
         [((ROWS // 2, D), BF)] * 2,
-        [((2, ROWS // 2, 1024), BF), ((4, ROWS // 2, 512), F32)],
-        where,
+        [((2, ROWS // 2, 1024), BF)],
         near(own),
         near(other),
         s_raising[None, :],
-        *(near(e) for e in extra),
         *(near(p) for p in pieces),
     )
-    (share,) = call(last_kernel, [piece], [], where, near(residual), *reduce_rows(keep, send))
-    return place(where, *spread_rows(share))
+    (shares,) = call(last_kernel, [((4, 48, D), BF)], [], where, reduce_rows(*sums), near(residual))
+    return place(where, *spread_rows(shares))
 
 
 def solution(mesh):

time: 261 us -> 211 us (0.81)
  waiting for transfers between devices: 83.7 us -> 44.1 us
  starting transfers between devices: 140 us -> 104 us
  blocking collectives: 0 us -> 28.4 us
    ppermute x12 -> x0, starting transfers between devices: 39.4 us -> none  [x_send(): return lax.ppermute(value, 'tp', [(t, t ^ 2 * mask) for t in range(8)])]
    all_to_all x0 -> x2, blocking collectives: none -> 28.4 us  [x_exchange(): lax.all_to_all(pieces, 'tp', 0, 0, axis_index_groups=X_GROUPS, tiled=True)]
    ppermute x12 -> x0, waiting for transfers between devices: 25.4 us -> none  [x_send(): return lax.ppermute(value, 'tp', [(t, t ^ 2 * mask) for t in range(8)])]
    ppermute x10 -> x4, waiting for transfers between devices: 39.9 us -> 16.7 us  [y_send(): return lax.ppermute(value, ZY, y_pairs(mask))]
    ppermute x10 -> x4, starting transfers between devices: 31.9 us -> 12 us  [y_send(): return lax.ppermute(value, ZY, y_pairs(mask))]
    all_to_all x0 -> x3, starting transfers between devices: none -> 12.7 us  [the longest x2 7.64 us: x_exchange(): lax.all_to_all(pieces, 'tp', 0, 0, axis_index_groups=X_GROUPS, tiled=True)]
    all_to_all x0 -> x3, waiting for transfers between devices: none -> 10.2 us  [the longest x2 10.2 us: x_exchange(): lax.all_to_all(pieces, 'tp', 0, 0, axis_index_groups=X_GROUPS, tiled=True)]
    ppermute x4, starting transfers between devices: 18.3 us -> 25.1 us  [core_swap(): return lax.ppermute(value, 'tp', [(t, t ^ 1) for t in range(8)])]
  transfers between devices with their start and end apart: 40 -> 25, of which waited for: 18 -> 8; matrix products, arithmetic and copies ran while one was open for 0% -> 1% of each run, Pallas kernels for 6% -> 8%
where the time goes in v1:
time: 211 us; the launch traced here: 210 us
  starting transfers between devices  104 us (49%)
  waiting for transfers between devices  44.1 us (21%)
  blocking collectives  28.4 us (13%)
  Pallas kernels  28 us (13%)
  local copies, waits for them, and re-layouts  5.06 us (2%)
    ppermute x14, starting transfers between devices, z_send(): return lax.ppermute(value, ZY, z_pairs(step))  54.4 us
    all_to_all x2, blocking collectives, x_exchange(): lax.all_to_all(pieces, 'tp', 0, 0, axis_index_groups=X_GROUPS, tiled=True)  28.4 us
    ppermute x4, starting transfers between devices, core_swap(): return lax.ppermute(value, 'tp', [(t, t ^ 1) for t in range(8)])  25.1 us
    pallas_call x9, Pallas kernels, call(): pl.pallas_call(kernel, out_shape=[pltpu.VMEM(s, t) for s, t in outs], in_...  22.7 us
    ppermute x4, waiting for transfers between devices, y_send(): return lax.ppermute(value, ZY, y_pairs(mask))  16.7 us
    ppermute x14, waiting for transfers between devices, z_send(): return lax.ppermute(value, ZY, z_pairs(step))  14.8 us
    ppermute x4, starting transfers between devices, y_send(): return lax.ppermute(value, ZY, y_pairs(mask))  12 us
    all_to_all x2, waiting for transfers between devices, x_exchange(): lax.all_to_all(pieces, 'tp', 0, 0, axis_index_groups=X_GROUPS, tiled=True)  10.2 us
  transfers between devices with their start and end apart: 25, of which 8 were waited for; matrix products, arithmetic and copies ran while one was open for 1% of the time, Pallas kernels for 8%

profile of v1, /device:TPU:1, one launch (start us, length us, event | category | flops | bytes accessed | tf_op | source)
XLA Modules:
  0.0 210.4 jit_solution(15825399252180402052)
XLA Ops:
  0.0 2.4 %cast.1 = (bf16[64,1152]{1,0:T(8,128)(2,1)S(1)}, bf16[4,64,2048]{2,1,0:T(8,128)(2,1)}) custom-call(f32[64,128]{1,0:T(8,128)} %refs_0_.1, f32[64,128]{1,0:T(8,128)} %refs_1_.1, f32[64,128]{1,0:T(8,128)} %refs_2_.1, f32[64,256]{1,0:T(8,128)} %refs_3_.1, f32[64,256]{1,0:T(8,128)} %refs_4_.1, f32[64,256]{1,0:T(8,128)} %bitcast.38, f32[64,1024]{1,0:T(8,128)} %refs_6_.1, ...), custom_call_target="tpu_custom_call" | custom-call | tf_op jit(solution)/shard_map/cast/pallas_call | solution.py:485
  2.4 5.0 %all-to-all-start.2 = ((bf16[4,64,2048]{2,1,0:T(8,128)(2,1)}), bf16[4,64,2048]{2,1,0:T(8,128)(2,1)}, u32[]{:S(2)}, u32[]{:S(2)}) async-start(bf16[4,64,2048]{2,1,0:T(8,128)(2,1)} %get-tuple-element.17), calls=%async_computation.2 | async-start | bytes 2097152 | tf_op jit(solution)/shard_map/all_to_all | solution.py:85
  7.4 5.0 %collective-permute-start.2 = (bf16[64,1152]{1,0:T(8,128)(2,1)S(1)}, bf16[64,1152]{1,0:T(8,128)(2,1)S(1)}, u32[]{:S(2)}, u32[]{:S(2)}) collective-permute-start(bf16[64,1152]{1,0:T(8,128)(2,1)S(1)} %get-tuple-element.13.refs_0_), channel_id=1, source_target_pairs={{0,64},{8,72},{16,80},{24,88},{32,96},{40,104},{48,112},{56,120},{... | collective-permute-start | bytes 442376 | tf_op jit(solution)/shard_map/ppermute | solution.py:31
  12.4 8.6 %collective-permute-start.3 = (bf16[64,1152]{1,0:T(8,128)(2,1)S(1)}, bf16[64,1152]{1,0:T(8,128)(2,1)S(1)}, u32[]{:S(2)}, u32[]{:S(2)}) collective-permute-start(bf16[64,1152]{1,0:T(8,128)(2,1)S(1)} %get-tuple-element.13.refs_0_), channel_id=1, source_target_pairs={{0,448},{8,456},{16,464},{24,472},{32,480},{40,488},{48,496},{56,5... | collective-permute-start | bytes 442376 | tf_op jit(solution)/shard_map/ppermute | solution.py:31
  21.0 2.6 %collective-permute-start = (bf16[64,1152]{1,0:T(8,128)(2,1)S(1)}, bf16[64,1152]{1,0:T(8,128)(2,1)S(1)}, u32[]{:S(2)}, u32[]{:S(2)}) collective-permute-start(bf16[64,1152]{1,0:T(8,128)(2,1)S(1)} %get-tuple-element.13.refs_0_), channel_id=1, source_target_pairs={{0,32},{8,40},{16,48},{24,56},{32,64},{40,72},{48,80},{56,88},{64,... | collective-permute-start | bytes 442376 | tf_op jit(solution)/shard_map/ppermute | solution.py:31
  23.6 3.8 %collective-permute-start.1 = (bf16[64,1152]{1,0:T(8,128)(2,1)S(1)}, bf16[64,1152]{1,0:T(8,128)(2,1)S(1)}, u32[]{:S(2)}, u32[]{:S(2)}) collective-permute-start(bf16[64,1152]{1,0:T(8,128)(2,1)S(1)} %get-tuple-element.13.refs_0_), channel_id=1, source_target_pairs={{0,480},{8,488},{16,496},{24,504},{32,0},{40,8},{48,16},{56,24},{6... | collective-permute-start | bytes 442376 | tf_op jit(solution)/shard_map/ppermute | solution.py:31
  27.5 0.0 collective-permute-done.2.refs_3_
  27.5 1.9 collective-permute-start.4
  29.4 1.9 collective-permute-start.6
  31.4 4.6 %collective-permute-start.5 = (bf16[64,1152]{1,0:T(8,128)(2,1)S(1)}, bf16[64,1152]{1,0:T(8,128)(2,1)S(1)}, u32[]{:S(2)}, u32[]{:S(2)}) collective-permute-start(bf16[64,1152]{1,0:T(8,128)(2,1)S(1)} %collective-permute-done.3.refs_4_), channel_id=1, source_target_pairs={{0,480},{8,488},{16,496},{24,504},{32,0},{40,8},{48,16},{56,24},{6... | collective-permute-start | bytes 442376 | tf_op jit(solution)/shard_map/ppermute | solution.py:31
  36.0 3.0 %collective-permute-done.6.refs_7_ = bf16[64,1152]{1,0:T(8,128)(2,1)S(1)} collective-permute-done((bf16[64,1152]{1,0:T(8,128)(2,1)S(1)}, bf16[64,1152]{1,0:T(8,128)(2,1)S(1)}, u32[]{:S(2)}, u32[]{:S(2)}) %collective-permute-start.6) | collective-permute-done | bytes 147488 | tf_op jit(solution)/shard_map/ppermute | solution.py:31
  38.9 0.1 shard_map.209.w0_ref
  39.0 0.0 copy-start.2
  39.0 4.3 %collective-permute-start.8 = (bf16[512,1152]{1,0:T(8,128)(2,1)S(1)}, bf16[512,1152]{1,0:T(8,128)(2,1)S(1)}, u32[]{:S(2)}, u32[]{:S(2)}) collective-permute-start(bf16[512,1152]{1,0:T(8,128)(2,1)S(1)} %shard_map.209.w0_ref), channel_id=1, source_target_pairs={{0,24},{8,16},{16,8},{24,0},{32,56},{40,48},{48,40},{56,32},{64,88... | collective-permute-start | bytes 3538952 | tf_op jit(solution)/shard_map/ppermute | solution.py:35
  43.4 1.9 collective-permute-start.7
  45.3 4.3 %collective-permute-start.13 = (bf16[256,2048]{1,0:T(8,128)(2,1)}, bf16[256,2048]{1,0:T(8,128)(2,1)}, u32[]{:S(2)}, u32[]{:S(2)}) collective-permute-start(bf16[256,2048]{1,0:T(8,128)(2,1)} %bitcast.20.refs_0_), channel_id=1, source_target_pairs={{0,32},{8,40},{16,48},{24,56},{32,64},{40,72},{48,80},{56,88},{64,... | collective-permute-start | bytes 3145736 | tf_op jit(solution)/shard_map/ppermute | solution.py:31
  49.6 16.7 %collective-permute-done.8.w3_ref = bf16[512,1152]{1,0:T(8,128)(2,1)S(1)} collective-permute-done((bf16[512,1152]{1,0:T(8,128)(2,1)S(1)}, bf16[512,1152]{1,0:T(8,128)(2,1)S(1)}, u32[]{:S(2)}, u32[]{:S(2)}) %collective-permute-start.8) | collective-permute-done | bytes 1179680 | tf_op jit(solution)/shard_map/ppermute | solution.py:35
  66.3 0.9 slice.9
  67.2 1.9 collective-permute-start.10
  69.2 0.9 slice.8
  70.0 3.8 %collective-permute-start.9 = (bf16[256,1152]{1,0:T(8,128)(2,1)}, bf16[256,1152]{1,0:T(8,128)(2,1)}, u32[]{:S(2)}, u32[]{:S(2)}) collective-permute-start(bf16[256,1152]{1,0:T(8,128)(2,1)} %slice.8), channel_id=1, source_target_pairs={{0,24},{8,16},{16,8},{24,0},{32,56},{40,48},{48,40},{56,32},{64,88... | collective-permute-start | bytes 1769480 | tf_op jit(solution)/shard_map/ppermute | solution.py:35
  73.9 6.7 %collective-permute-start.14 = (bf16[256,2048]{1,0:T(8,128)(2,1)}, bf16[256,2048]{1,0:T(8,128)(2,1)}, u32[]{:S(2)}, u32[]{:S(2)}) collective-permute-start(bf16[256,2048]{1,0:T(8,128)(2,1)} %bitcast.20.refs_0_), channel_id=1, source_target_pairs={{0,480},{8,488},{16,496},{24,504},{32,0},{40,8},{48,16},{56,24},{6... | collective-permute-start | bytes 3145736 | tf_op jit(solution)/shard_map/ppermute | solution.py:31
  80.6 1.9 collective-permute-start.15
  82.5 0.1 pad_add_fusion.where_ref
  82.6 1.4 copy-done
  84.0 2.7 %shard_map.208.x_ref = bf16[384,2048]{1,0:T(8,128)(2,1)S(1)} custom-call(s32[4]{0:T(128)S(1)} %pad_add_fusion.where_ref, bf16[384,2048]{1,0:T(8,128)(2,1)S(1)} %copy-done, f32[1,2048]{1,0:T(1,128)S(1)} %bitcast.26), custom_call_target="tpu_custom_call" | custom-call | tf_op jit(solution)/shard_map/pallas_call | solution.py:408
  86.8 0.0 copy-start.5
  86.8 0.0 copy-start.6
  86.8 0.0 copy-start.7
  86.8 0.0 copy-start.8
  86.8 0.0 copy-start.9
  86.8 0.0 copy-start.10
  86.8 0.0 copy-start.11
  86.8 0.0 copy-start.12
  86.9 2.3 %shard_map.210.early_ref = f32[384,896]{1,0:T(8,128)S(1)} custom-call(bf16[384,2048]{1,0:T(8,128)(2,1)S(1)} %shard_map.208.x_ref, bf16[512,1152]{1,0:T(8,128)(2,1)S(1)} %shard_map.209.w0_ref, bf16[512,1152]{1,0:T(8,128)(2,1)S(1)} %collective-permute-done.7.w1_ref, bf16[512,1152]{1,0:T(8,128)(2,1)S(1)} %collective-permute-done.8.w3_ref), custom_call_target="tpu_custom_call" | custom-call | tf_op jit(solution)/shard_map/pallas_call | solution.py:408
  89.3 7.3 %shard_map.211 = (bf16[192,2048]{1,0:T(8,128)(2,1)S(1)}, bf16[192,2048]{1,0:T(8,128)(2,1)S(1)}) custom-call(s32[4]{0:T(128)S(1)} %pad_add_fusion.where_ref, bf16[384,2048]{1,0:T(8,128)(2,1)S(1)} %shard_map.208.x_ref, f32[384,896]{1,0:T(8,128)S(1)} %shard_map.210.early_ref, bf16[512,1152]{1,0:T(8,128)(2,1)S(1)} %shard_map.209.w0_ref, ...), custom_call_target="tpu_custom_call" | custom-call | tf_op jit(solution)/shard_map/pallas_call | solution.py:408
  96.6 5.7 %collective-permute-start.11 = (bf16[192,2048]{1,0:T(8,128)(2,1)S(1)}, bf16[192,2048]{1,0:T(8,128)(2,1)S(1)}, u32[]{:S(2)}, u32[]{:S(2)}) collective-permute-start(bf16[192,2048]{1,0:T(8,128)(2,1)S(1)} %get-tuple-element.15), channel_id=1, source_target_pairs={{0,1},{1,0},{2,3},{3,2},{4,5},{5,4},{6,7},{7,6},{8,9},{9,8},{10,11... | collective-permute-start | bytes 2359304 | tf_op jit(solution)/shard_map/ppermute | solution.py:39
  102.3 4.8 %collective-permute-start.16 = (bf16[256,2048]{1,0:T(8,128)(2,1)}, bf16[256,2048]{1,0:T(8,128)(2,1)S(1)}, u32[]{:S(2)}, u32[]{:S(2)}) collective-permute-start(bf16[256,2048]{1,0:T(8,128)(2,1)} %collective-permute-done.14.refs_2_), channel_id=1, source_target_pairs={{0,480},{8,488},{16,496},{24,504},{32,0},{40,8},{48,16},{56,24},{6... | collective-permute-start | bytes 3145736 | tf_op jit(solution)/shard_map/ppermute | solution.py:31
  107.2 1.9 collective-permute-start.17
  109.1 1.1 shard_map.212
  110.2 4.1 %all-to-all-start = ((bf16[4,48,2048]{2,1,0:T(8,128)(2,1)}), bf16[4,48,2048]{2,1,0:T(8,128)(2,1)S(1)}, u32[]{:S(2)}, u32[]{:S(2)}) async-start(bf16[4,48,2048]{2,1,0:T(8,128)(2,1)} %shard_map.212), calls=%async_computation | async-start | bytes 1572864 | tf_op jit(solution)/shard_map/all_to_all | solution.py:46
  114.3 1.0 constant_dynamic-slice_fusion.x_ref
  115.3 8.1 %all-to-all-done.parts_ref = bf16[4,48,2048]{2,1,0:T(8,128)(2,1)S(1)} async-done(((bf16[4,48,2048]{2,1,0:T(8,128)(2,1)}), bf16[4,48,2048]{2,1,0:T(8,128)(2,1)S(1)}, u32[]{:S(2)}, u32[]{:S(2)}) %all-to-all-start) | async-done | bytes 786464 | tf_op jit(solution)/shard_map/all_to_all | solution.py:46
  123.4 1.0 shard_map.213
  124.4 0.0 copy-start.1
  124.4 0.9 copy-done.1
  125.3 3.5 %all-to-all-start.1 = ((bf16[4,48,2048]{2,1,0:T(8,128)(2,1)}), bf16[4,48,2048]{2,1,0:T(8,128)(2,1)S(1)}, u32[]{:S(2)}, u32[]{:S(2)}) async-start(bf16[4,48,2048]{2,1,0:T(8,128)(2,1)} %copy-done.1), calls=%async_computation.1 | async-start | bytes 1572864 | tf_op jit(solution)/shard_map/all_to_all | solution.py:46
  128.8 4.3 %collective-permute-start.18 = (bf16[256,2048]{1,0:T(8,128)(2,1)S(1)}, bf16[256,2048]{1,0:T(8,128)(2,1)}, u32[]{:S(2)}, u32[]{:S(2)}) collective-permute-start(bf16[256,2048]{1,0:T(8,128)(2,1)S(1)} %collective-permute-done.16.refs_4_), channel_id=1, source_target_pairs={{0,480},{8,488},{16,496},{24,504},{32,0},{40,8},{48,16},{56,24},{6... | collective-permute-start | bytes 3145736 | tf_op jit(solution)/shard_map/ppermute | solution.py:31
  133.1 1.9 collective-permute-start.19
  135.0 2.1 all-to-all-done.1
  137.1 7.4 %collective-permute-start.12 = (bf16[192,2048]{1,0:T(8,128)(2,1)S(1)}, bf16[192,2048]{1,0:T(8,128)(2,1)S(1)}, u32[]{:S(2)}, u32[]{:S(2)}) collective-permute-start(bf16[192,2048]{1,0:T(8,128)(2,1)S(1)} %bitcast.22), channel_id=1, source_target_pairs={{0,1},{1,0},{2,3},{3,2},{4,5},{5,4},{6,7},{7,6},{8,9},{9,8},{10,11... | collective-permute-start | bytes 2359304 | tf_op jit(solution)/shard_map/ppermute | solution.py:39
  144.5 6.9 %collective-permute-done.18.refs_6_ = bf16[256,2048]{1,0:T(8,128)(2,1)} collective-permute-done((bf16[256,2048]{1,0:T(8,128)(2,1)S(1)}, bf16[256,2048]{1,0:T(8,128)(2,1)}, u32[]{:S(2)}, u32[]{:S(2)}) %collective-permute-start.18) | collective-permute-done | bytes 1048608 | tf_op jit(solution)/shard_map/ppermute | solution.py:31
  151.3 5.0 %collective-permute-done.19.refs_7_ = bf16[256,2048]{1,0:T(8,128)(2,1)} collective-permute-done((bf16[256,2048]{1,0:T(8,128)(2,1)S(1)}, bf16[256,2048]{1,0:T(8,128)(2,1)}, u32[]{:S(2)}, u32[]{:S(2)}) %collective-permute-start.19) | collective-permute-done | bytes 1048608 | tf_op jit(solution)/shard_map/ppermute | solution.py:31
  156.3 7.4 %shard_map.214 = (bf16[192,2048]{1,0:T(8,128)(2,1)S(1)}, bf16[192,2048]{1,0:T(8,128)(2,1)S(1)}) custom-call(bf16[192,2048]{1,0:T(8,128)(2,1)S(1)} %bitcast.23, bf16[192,2048]{1,0:T(8,128)(2,1)S(1)} %collective-permute-done.12.other_ref, f32[1,1024]{1,0:T(1,128)S(1)} %bitcast.28, bf16[256,2048]{1,0:T(8,128)(2,1)} %bitcast.20.refs_0_, ...), custom_call_target="tpu_custom_call" | custom-call | tf_op jit(solution)/shard_map/pallas_call | solution.py:408
  163.7 7.5 %collective-permute-start.20 = (bf16[192,2048]{1,0:T(8,128)(2,1)S(1)}, bf16[192,2048]{1,0:T(8,128)(2,1)S(1)}, u32[]{:S(2)}, u32[]{:S(2)}) collective-permute-start(bf16[192,2048]{1,0:T(8,128)(2,1)S(1)} %get-tuple-element.19), channel_id=1, source_target_pairs={{0,1},{1,0},{2,3},{3,2},{4,5},{5,4},{6,7},{7,6},{8,9},{9,8},{10,11... | collective-permute-start | bytes 2359304 | tf_op jit(solution)/shard_map/ppermute | solution.py:39
  171.2 1.9 collective-permute-done.20.got_ref
  173.1 0.2 shard_map.215
  173.2 15.4 %all_to_all.25.parts_ref = bf16[4,48,2048]{2,1,0:T(8,128)(2,1)S(1)} all-to-all(bf16[4,48,2048]{2,1,0:T(8,128)(2,1)S(1)} %shard_map.215), channel_id=1, replica_groups={{0,2,4,6},{1,3,5,7},{8,10,12,14},{9,11,13,15},{16,18,20,22},{17,19,21,2..., dimensions={0} | all-to-all | bytes 1572864 | tf_op jit(solution)/shard_map/all_to_all | solution.py:46
  188.7 0.7 shard_map.216
  189.3 13.0 %all_to_all.26 = bf16[4,48,2048]{2,1,0:T(8,128)(2,1)S(1)} all-to-all(bf16[4,48,2048]{2,1,0:T(8,128)(2,1)S(1)} %shard_map.216), channel_id=1, replica_groups={{0,2,4,6},{1,3,5,7},{8,10,12,14},{9,11,13,15},{16,18,20,22},{17,19,21,2..., dimensions={0} | all-to-all | bytes 1572864 | tf_op jit(solution)/shard_map/all_to_all | solution.py:46
  202.3 4.6 %collective-permute-start.21 = (bf16[192,2048]{1,0:T(8,128)(2,1)S(1)}, bf16[192,2048]{1,0:T(8,128)(2,1)S(1)}, u32[]{:S(2)}, u32[]{:S(2)}) collective-permute-start(bf16[192,2048]{1,0:T(8,128)(2,1)S(1)} %bitcast.24), channel_id=1, source_target_pairs={{0,1},{1,0},{2,3},{3,2},{4,5},{5,4},{6,7},{7,6},{8,9},{9,8},{10,11... | collective-permute-start | bytes 2359304 | tf_op jit(solution)/shard_map/ppermute | solution.py:39
  206.9 1.4 place_own.1.held_ref
  208.3 0.4 collective-permute-done.21.other_ref
  208.8 1.4 place_other.1
  (30 shorter events, 0.1 us)
Async XLA Ops:
  2.4 42.9 %all-to-all-start.2 = ((bf16[4,64,2048]{2,1,0:T(8,128)(2,1)}), bf16[4,64,2048]{2,1,0:T(8,128)(2,1)}, u32[]{:S(2)}, u32[]{:S(2)}) async-start(bf16[4,64,2048]{2,1,0:T(8,128)(2,1)} %get-tuple-element.17), calls=%async_computation.2 | async-start | bytes 2097152 | tf_op jit(solution)/shard_map/all_to_all | solution.py:85
  7.4 20.1 %collective-permute-start.2 = (bf16[64,1152]{1,0:T(8,128)(2,1)S(1)}, bf16[64,1152]{1,0:T(8,128)(2,1)S(1)}, u32[]{:S(2)}, u32[]{:S(2)}) collective-permute-start(bf16[64,1152]{1,0:T(8,128)(2,1)S(1)} %get-tuple-element.13.refs_0_), channel_id=1, source_target_pairs={{0,64},{8,72},{16,80},{24,88},{32,96},{40,104},{48,112},{56,120},{... | collective-permute-start | bytes 442376 | tf_op jit(solution)/shard_map/ppermute | solution.py:31
  12.4 19.0 %collective-permute-start.3 = (bf16[64,1152]{1,0:T(8,128)(2,1)S(1)}, bf16[64,1152]{1,0:T(8,128)(2,1)S(1)}, u32[]{:S(2)}, u32[]{:S(2)}) collective-permute-start(bf16[64,1152]{1,0:T(8,128)(2,1)S(1)} %get-tuple-element.13.refs_0_), channel_id=1, source_target_pairs={{0,448},{8,456},{16,464},{24,472},{32,480},{40,488},{48,496},{56,5... | collective-permute-start | bytes 442376 | tf_op jit(solution)/shard_map/ppermute | solution.py:31
  21.0 15.0 %collective-permute-start = (bf16[64,1152]{1,0:T(8,128)(2,1)S(1)}, bf16[64,1152]{1,0:T(8,128)(2,1)S(1)}, u32[]{:S(2)}, u32[]{:S(2)}) collective-permute-start(bf16[64,1152]{1,0:T(8,128)(2,1)S(1)} %get-tuple-element.13.refs_0_), channel_id=1, source_target_pairs={{0,32},{8,40},{16,48},{24,56},{32,64},{40,72},{48,80},{56,88},{64,... | collective-permute-start | bytes 442376 | tf_op jit(solution)/shard_map/ppermute | solution.py:31
  23.6 12.3 %collective-permute-start.1 = (bf16[64,1152]{1,0:T(8,128)(2,1)S(1)}, bf16[64,1152]{1,0:T(8,128)(2,1)S(1)}, u32[]{:S(2)}, u32[]{:S(2)}) collective-permute-start(bf16[64,1152]{1,0:T(8,128)(2,1)S(1)} %get-tuple-element.13.refs_0_), channel_id=1, source_target_pairs={{0,480},{8,488},{16,496},{24,504},{32,0},{40,8},{48,16},{56,24},{6... | collective-permute-start | bytes 442376 | tf_op jit(solution)/shard_map/ppermute | solution.py:31
  27.5 8.5 %collective-permute-start.4 = (bf16[64,1152]{1,0:T(8,128)(2,1)S(1)}, bf16[64,1152]{1,0:T(8,128)(2,1)S(1)}, u32[]{:S(2)}, u32[]{:S(2)}) collective-permute-start(bf16[64,1152]{1,0:T(8,128)(2,1)S(1)} %collective-permute-done.2.refs_3_), channel_id=1, source_target_pairs={{0,32},{8,40},{16,48},{24,56},{32,64},{40,72},{48,80},{56,88},{64,... | collective-permute-start | bytes 442376 | tf_op jit(solution)/shard_map/ppermute | solution.py:31
  29.4 9.5 %collective-permute-start.6 = (bf16[64,1152]{1,0:T(8,128)(2,1)S(1)}, bf16[64,1152]{1,0:T(8,128)(2,1)S(1)}, u32[]{:S(2)}, u32[]{:S(2)}) collective-permute-start(bf16[64,1152]{1,0:T(8,128)(2,1)S(1)} %collective-permute-done.2.refs_3_), channel_id=1, source_target_pairs={{0,64},{8,72},{16,80},{24,88},{32,96},{40,104},{48,112},{56,120},{... | collective-permute-start | bytes 442376 | tf_op jit(solution)/shard_map/ppermute | solution.py:31
  31.4 7.6 %collective-permute-start.5 = (bf16[64,1152]{1,0:T(8,128)(2,1)S(1)}, bf16[64,1152]{1,0:T(8,128)(2,1)S(1)}, u32[]{:S(2)}, u32[]{:S(2)}) collective-permute-start(bf16[64,1152]{1,0:T(8,128)(2,1)S(1)} %collective-permute-done.3.refs_4_), channel_id=1, source_target_pairs={{0,480},{8,488},{16,496},{24,504},{32,0},{40,8},{48,16},{56,24},{6... | collective-permute-start | bytes 442376 | tf_op jit(solution)/shard_map/ppermute | solution.py:31
  39.0 43.6 %copy-start.2 = (f32[2048]{0:T(1024)S(1)}, f32[2048]{0:T(1024)}, u32[]{:S(2)}) copy-start(f32[2048]{0:T(1024)} %param.23) | copy-start | bytes 24580
  39.0 27.3 %collective-permute-start.8 = (bf16[512,1152]{1,0:T(8,128)(2,1)S(1)}, bf16[512,1152]{1,0:T(8,128)(2,1)S(1)}, u32[]{:S(2)}, u32[]{:S(2)}) collective-permute-start(bf16[512,1152]{1,0:T(8,128)(2,1)S(1)} %shard_map.209.w0_ref), channel_id=1, source_target_pairs={{0,24},{8,16},{16,8},{24,0},{32,56},{40,48},{48,40},{56,32},{64,88... | collective-permute-start | bytes 3538952 | tf_op jit(solution)/shard_map/ppermute | solution.py:35
  43.4 25.8 %collective-permute-start.7 = (bf16[512,1152]{1,0:T(8,128)(2,1)S(1)}, bf16[512,1152]{1,0:T(8,128)(2,1)S(1)}, u32[]{:S(2)}, u32[]{:S(2)}) collective-permute-start(bf16[512,1152]{1,0:T(8,128)(2,1)S(1)} %shard_map.209.w0_ref), channel_id=1, source_target_pairs={{0,8},{8,0},{16,24},{24,16},{32,40},{40,32},{48,56},{56,48},{64,72... | collective-permute-start | bytes 3538952 | tf_op jit(solution)/shard_map/ppermute | solution.py:35
  45.3 35.3 %collective-permute-start.13 = (bf16[256,2048]{1,0:T(8,128)(2,1)}, bf16[256,2048]{1,0:T(8,128)(2,1)}, u32[]{:S(2)}, u32[]{:S(2)}) collective-permute-start(bf16[256,2048]{1,0:T(8,128)(2,1)} %bitcast.20.refs_0_), channel_id=1, source_target_pairs={{0,32},{8,40},{16,48},{24,56},{32,64},{40,72},{48,80},{56,88},{64,... | collective-permute-start | bytes 3145736 | tf_op jit(solution)/shard_map/ppermute | solution.py:31
  67.2 21.9 %collective-permute-start.10 = (bf16[256,1152]{1,0:T(8,128)(2,1)}, bf16[256,1152]{1,0:T(8,128)(2,1)}, u32[]{:S(2)}, u32[]{:S(2)}) collective-permute-start(bf16[256,1152]{1,0:T(8,128)(2,1)} %slice.9), channel_id=1, source_target_pairs={{0,8},{8,0},{16,24},{24,16},{32,40},{40,32},{48,56},{56,48},{64,72... | collective-permute-start | bytes 1769480 | tf_op jit(solution)/shard_map/ppermute | solution.py:35
  70.0 19.1 %collective-permute-start.9 = (bf16[256,1152]{1,0:T(8,128)(2,1)}, bf16[256,1152]{1,0:T(8,128)(2,1)}, u32[]{:S(2)}, u32[]{:S(2)}) collective-permute-start(bf16[256,1152]{1,0:T(8,128)(2,1)} %slice.8), channel_id=1, source_target_pairs={{0,24},{8,16},{16,8},{24,0},{32,56},{40,48},{48,40},{56,32},{64,88... | collective-permute-start | bytes 1769480 | tf_op jit(solution)/shard_map/ppermute | solution.py:35
  73.9 28.4 %collective-permute-start.14 = (bf16[256,2048]{1,0:T(8,128)(2,1)}, bf16[256,2048]{1,0:T(8,128)(2,1)}, u32[]{:S(2)}, u32[]{:S(2)}) collective-permute-start(bf16[256,2048]{1,0:T(8,128)(2,1)} %bitcast.20.refs_0_), channel_id=1, source_target_pairs={{0,480},{8,488},{16,496},{24,504},{32,0},{40,8},{48,16},{56,24},{6... | collective-permute-start | bytes 3145736 | tf_op jit(solution)/shard_map/ppermute | solution.py:31
  80.6 26.5 %collective-permute-start.15 = (bf16[256,2048]{1,0:T(8,128)(2,1)}, bf16[256,2048]{1,0:T(8,128)(2,1)}, u32[]{:S(2)}, u32[]{:S(2)}) collective-permute-start(bf16[256,2048]{1,0:T(8,128)(2,1)} %collective-permute-done.13.refs_1_), channel_id=1, source_target_pairs={{0,32},{8,40},{16,48},{24,56},{32,64},{40,72},{48,80},{56,88},{64,... | collective-permute-start | bytes 3145736 | tf_op jit(solution)/shard_map/ppermute | solution.py:31
  82.6 1.4 copy-start
  86.8 2.4 %copy-start.5 = (f32[384,1]{0,1:T(1,128)S(1)}, f32[384,1]{0,1:T(1,128)}, u32[]{:S(2)}) copy-start(f32[384,1]{0,1:T(1,128)} %param.31) | copy-start | bytes 4612
  86.8 2.4 %copy-start.6 = (f32[256]{0:T(256)S(1)}, f32[256]{0:T(256)}, u32[]{:S(2)}) copy-start(f32[256]{0:T(256)} %param.33) | copy-start | bytes 3076
  86.8 2.4 %copy-start.7 = (f32[256]{0:T(256)S(1)}, f32[256]{0:T(256)}, u32[]{:S(2)}) copy-start(f32[256]{0:T(256)} %param.35) | copy-start | bytes 3076
  86.8 2.4 %copy-start.8 = (f32[256]{0:T(256)S(1)}, f32[256]{0:T(256)}, u32[]{:S(2)}) copy-start(f32[256]{0:T(256)} %param.36) | copy-start | bytes 3076
  86.8 2.4 %copy-start.9 = (f32[128]{0:T(128)S(1)}, f32[128]{0:T(128)}, u32[]{:S(2)}) copy-start(f32[128]{0:T(128)} %param.25) | copy-start | bytes 1540
  86.8 2.4 %copy-start.10 = (f32[128]{0:T(128)S(1)}, f32[128]{0:T(128)}, u32[]{:S(2)}) copy-start(f32[128]{0:T(128)} %param.27) | copy-start | bytes 1540
  86.8 2.4 %copy-start.11 = (f32[128]{0:T(128)S(1)}, f32[128]{0:T(128)}, u32[]{:S(2)}) copy-start(f32[128]{0:T(128)} %param.29) | copy-start | bytes 1540
  86.8 2.4 %copy-start.12 = (f32[128]{0:T(128)S(1)}, f32[128]{0:T(128)}, u32[]{:S(2)}) copy-start(f32[128]{0:T(128)} %param.30) | copy-start | bytes 1540
  96.6 12.5 %collective-permute-start.11 = (bf16[192,2048]{1,0:T(8,128)(2,1)S(1)}, bf16[192,2048]{1,0:T(8,128)(2,1)S(1)}, u32[]{:S(2)}, u32[]{:S(2)}) collective-permute-start(bf16[192,2048]{1,0:T(8,128)(2,1)S(1)} %get-tuple-element.15), channel_id=1, source_target_pairs={{0,1},{1,0},{2,3},{3,2},{4,5},{5,4},{6,7},{7,6},{8,9},{9,8},{10,11... | collective-permute-start | bytes 2359304 | tf_op jit(solution)/shard_map/ppermute | solution.py:39
  102.3 26.5 %collective-permute-start.16 = (bf16[256,2048]{1,0:T(8,128)(2,1)}, bf16[256,2048]{1,0:T(8,128)(2,1)S(1)}, u32[]{:S(2)}, u32[]{:S(2)}) collective-permute-start(bf16[256,2048]{1,0:T(8,128)(2,1)} %collective-permute-done.14.refs_2_), channel_id=1, source_target_pairs={{0,480},{8,488},{16,496},{24,504},{32,0},{40,8},{48,16},{56,24},{6... | collective-permute-start | bytes 3145736 | tf_op jit(solution)/shard_map/ppermute | solution.py:31
  107.2 25.9 %collective-permute-start.17 = (bf16[256,2048]{1,0:T(8,128)(2,1)}, bf16[256,2048]{1,0:T(8,128)(2,1)S(1)}, u32[]{:S(2)}, u32[]{:S(2)}) collective-permute-start(bf16[256,2048]{1,0:T(8,128)(2,1)} %collective-permute-done.15.refs_3_), channel_id=1, source_target_pairs={{0,32},{8,40},{16,48},{24,56},{32,64},{40,72},{48,80},{56,88},{64,... | collective-permute-start | bytes 3145736 | tf_op jit(solution)/shard_map/ppermute | solution.py:31
  110.2 13.2 %copy-start.3 = (f32[2048]{0:T(1024)S(1)}, f32[2048]{0:T(1024)}, u32[]{:S(2)}) copy-start(f32[2048]{0:T(1024)} %param.39) | copy-start | bytes 24580
  110.2 13.2 %all-to-all-start = ((bf16[4,48,2048]{2,1,0:T(8,128)(2,1)}), bf16[4,48,2048]{2,1,0:T(8,128)(2,1)S(1)}, u32[]{:S(2)}, u32[]{:S(2)}) async-start(bf16[4,48,2048]{2,1,0:T(8,128)(2,1)} %shard_map.212), calls=%async_computation | async-start | bytes 1572864 | tf_op jit(solution)/shard_map/all_to_all | solution.py:46
  114.3 42.0 %copy-start.4 = (f32[1024]{0:T(1024)S(1)}, f32[1024]{0:T(1024)}, u32[]{:S(2)}) copy-start(f32[1024]{0:T(1024)} %param.41) | copy-start | bytes 12292
  124.4 0.9 copy-start.1
  125.3 11.8 %all-to-all-start.1 = ((bf16[4,48,2048]{2,1,0:T(8,128)(2,1)}), bf16[4,48,2048]{2,1,0:T(8,128)(2,1)S(1)}, u32[]{:S(2)}, u32[]{:S(2)}) async-start(bf16[4,48,2048]{2,1,0:T(8,128)(2,1)} %copy-done.1), calls=%async_computation.1 | async-start | bytes 1572864 | tf_op jit(solution)/shard_map/all_to_all | solution.py:46
  128.8 22.6 %collective-permute-start.18 = (bf16[256,2048]{1,0:T(8,128)(2,1)S(1)}, bf16[256,2048]{1,0:T(8,128)(2,1)}, u32[]{:S(2)}, u32[]{:S(2)}) collective-permute-start(bf16[256,2048]{1,0:T(8,128)(2,1)S(1)} %collective-permute-done.16.refs_4_), channel_id=1, source_target_pairs={{0,480},{8,488},{16,496},{24,504},{32,0},{40,8},{48,16},{56,24},{6... | collective-permute-start | bytes 3145736 | tf_op jit(solution)/shard_map/ppermute | solution.py:31
  133.1 23.2 %collective-permute-start.19 = (bf16[256,2048]{1,0:T(8,128)(2,1)S(1)}, bf16[256,2048]{1,0:T(8,128)(2,1)}, u32[]{:S(2)}, u32[]{:S(2)}) collective-permute-start(bf16[256,2048]{1,0:T(8,128)(2,1)S(1)} %collective-permute-done.17.refs_5_), channel_id=1, source_target_pairs={{0,32},{8,40},{16,48},{24,56},{32,64},{40,72},{48,80},{56,88},{64,... | collective-permute-start | bytes 3145736 | tf_op jit(solution)/shard_map/ppermute | solution.py:31
  137.1 14.3 %collective-permute-start.12 = (bf16[192,2048]{1,0:T(8,128)(2,1)S(1)}, bf16[192,2048]{1,0:T(8,128)(2,1)S(1)}, u32[]{:S(2)}, u32[]{:S(2)}) collective-permute-start(bf16[192,2048]{1,0:T(8,128)(2,1)S(1)} %bitcast.22), channel_id=1, source_target_pairs={{0,1},{1,0},{2,3},{3,2},{4,5},{5,4},{6,7},{7,6},{8,9},{9,8},{10,11... | collective-permute-start | bytes 2359304 | tf_op jit(solution)/shard_map/ppermute | solution.py:39
  163.7 9.4 %collective-permute-start.20 = (bf16[192,2048]{1,0:T(8,128)(2,1)S(1)}, bf16[192,2048]{1,0:T(8,128)(2,1)S(1)}, u32[]{:S(2)}, u32[]{:S(2)}) collective-permute-start(bf16[192,2048]{1,0:T(8,128)(2,1)S(1)} %get-tuple-element.19), channel_id=1, source_target_pairs={{0,1},{1,0},{2,3},{3,2},{4,5},{5,4},{6,7},{7,6},{8,9},{9,8},{10,11... | collective-permute-start | bytes 2359304 | tf_op jit(solution)/shard_map/ppermute | solution.py:39
  202.3 6.5 %collective-permute-start.21 = (bf16[192,2048]{1,0:T(8,128)(2,1)S(1)}, bf16[192,2048]{1,0:T(8,128)(2,1)S(1)}, u32[]{:S(2)}, u32[]{:S(2)}) collective-permute-start(bf16[192,2048]{1,0:T(8,128)(2,1)S(1)} %bitcast.24), channel_id=1, source_target_pairs={{0,1},{1,0},{2,3},{3,2},{4,5},{5,4},{6,7},{7,6},{8,9},{9,8},{10,11... | collective-permute-start | bytes 2359304 | tf_op jit(solution)/shard_map/ppermute | solution.py:39
